TPU v7x, 32 devices: a whole 2x2x4 slice. The times are simulated.
32 devices in a mesh: sp: 16 (over z, y, x), tp: 2 (over core).
Axes of the slice: x: 2, y: 2, z: 4, core: 2. Of those that a mesh axis runs over, the one named last changes fastest.
Arguments:
- tokens: bfloat16 [6144, 4096], P(('sp', 'tp')), may hold values from -6 to 6
- norm_gain: float32 [4096], replicated, may hold values from 0.1 to 1.9
- conv_val_w: bfloat16 [4096, 1024], P('sp', 'tp'), may hold values from -0.09375 to 0.09375
- conv_gate_w: bfloat16 [4096, 1024], P('sp', 'tp'), may hold values from -0.09375 to 0.09375
- rec_gate_w: bfloat16 [4096, 1536], P('sp', 'tp'), may hold values from -0.09375 to 0.09375
- rec_in_w: bfloat16 [4096, 1536], P('sp', 'tp'), may hold values from -0.09375 to 0.09375
- conv_taps: bfloat16 [31, 1024], P(None, 'tp'), may hold values from -3 to 3
- conv_bias: float32 [1024], P('tp'), may hold values from 1 to 15
- conv_gain: float32 [1024], P('tp'), may hold values from 0.1 to 1.9
- short_taps: bfloat16 [4, 1536], P(None, 'tp'), may hold values from -3 to 3
- decay_map: bfloat16 [24, 64, 64], P('tp'), may hold values from -0.75 to 0.75
- input_map: bfloat16 [24, 64, 64], P('tp'), may hold values from -0.75 to 0.75
- decay_base: float32 [1536], P('tp'), may hold values from 3.5 to 17
- decay_jump: float32 [6144, 1536], P('sp', 'tp'), may hold values from -1.5 to 0
- out_conv_w: bfloat16 [1024, 4096], P('tp', 'sp'), may hold values from -0.125 to 0.125
- out_rec_w: bfloat16 [1536, 4096], P('tp', 'sp'), may hold values from -0.125 to 0.125
Outputs:
- mixed: bfloat16 [6144, 4096], P(('sp', 'tp'))
All inputs are finite; a program needn't handle non-finite values.
Results may differ from a plain program's by a relative error of at most 0.015.
Values may be sent and summed in bfloat16 or wider, within the bound.
A program may use at most 128 MiB of HBM per device.

v0:
```python
import jax
import jax.numpy as jnp
from jax import lax
from jax.sharding import PartitionSpec as P

CONV_WIDTH = 1024


RATE_SCALE = 8.0


def passed_along(value, axis, by):
    count = lax.axis_size(axis)
    pairs = [(i, i + by) for i in range(count) if 0 <= i + by < count]
    return lax.ppermute(value, axis, pairs)


def prefix(part, axis, combine, identity):
    place = lax.axis_index(axis)
    gathered = jax.tree.map(lambda a: lax.all_gather(a, axis), part)
    state = jax.tree.map(lambda a, e: jnp.zeros_like(a) + jnp.asarray(e, a.dtype), part, identity)

    def one(step, state):
        return combine(
            state, jax.tree.map(lambda a: lax.dynamic_index_in_dim(a, step, 0, False), gathered)
        )

    return lax.fori_loop(0, place, one, state)


def norm_rows(values, gain):
    widened = values.astype(jnp.float32)
    inverse = lax.rsqrt(jnp.mean(widened * widened, axis=-1, keepdims=True) + 1e-06)
    return (widened * inverse * gain).astype(jnp.bfloat16)


def causal_window(edge, current, weights):
    extended = jnp.concatenate([edge, current], axis=0).astype(jnp.float32)
    taps_wide = weights.astype(jnp.float32)
    length = current.shape[0]
    result = jnp.zeros((length, current.shape[1]), jnp.float32)
    for lag_index in range(weights.shape[0]):
        result = result + taps_wide[lag_index][None, :] * extended[lag_index : lag_index + length]
    return result


def chain_step(earlier, latter):
    return (earlier[0] * latter[0], latter[0] * earlier[1] + latter[1])


def glu_of(conv_val, conv_gate):
    return (conv_val.astype(jnp.float32) * jax.nn.sigmoid(conv_gate.astype(jnp.float32))).astype(
        jnp.bfloat16
    )


def shards(
    tokens,
    norm_gain,
    conv_val_w,
    conv_gate_w,
    rec_gate_w,
    rec_in_w,
    conv_taps,
    conv_bias,
    conv_gain,
    short_taps,
    decay_map,
    input_map,
    decay_base,
    decay_jump,
    out_conv_w,
    out_rec_w,
):
    rec_cols = rec_in_w.shape[1]
    conv_lags = conv_taps.shape[0] - 1
    short_lags = short_taps.shape[0] - 1
    normed = norm_rows(tokens, norm_gain)
    val_full, gate_full = (
        lax.all_gather(conv_val_w, "sp", axis=0, tiled=True),
        lax.all_gather(conv_gate_w, "sp", axis=0, tiled=True),
    )
    all_rows = lax.all_gather(normed, "tp", axis=0, tiled=True)
    conv_val = jnp.dot(all_rows, val_full, preferred_element_type=jnp.float32).astype(jnp.bfloat16)
    conv_gate = jnp.dot(all_rows, gate_full, preferred_element_type=jnp.float32).astype(
        jnp.bfloat16
    )
    glu = glu_of(conv_val, conv_gate)
    conv_edge = passed_along(glu[-conv_lags:], "sp", 1)
    rgate_full, rin_full = (
        lax.all_gather(rec_gate_w, "sp", axis=0, tiled=True),
        lax.all_gather(rec_in_w, "sp", axis=0, tiled=True),
    )
    rec_gate = jnp.dot(all_rows, rgate_full, preferred_element_type=jnp.float32).astype(
        jnp.bfloat16
    )
    rec_in = jnp.dot(all_rows, rin_full, preferred_element_type=jnp.float32).astype(jnp.bfloat16)
    rec_edge = passed_along(rec_in[-short_lags:], "sp", 1)
    filtered = causal_window(conv_edge, glu, conv_taps) + conv_bias[None, :]
    row_total = lax.psum(jnp.sum(filtered, axis=1), "tp")
    centered = filtered - (row_total / CONV_WIDTH)[:, None]
    spread = lax.psum(jnp.sum(centered * centered, axis=1), "tp") / CONV_WIDTH
    conv_out = jax.nn.silu(centered * lax.rsqrt(spread + 1e-05)[:, None] * conv_gain).astype(
        jnp.bfloat16
    )
    smoothed = causal_window(rec_edge, rec_in, short_taps).astype(jnp.bfloat16)
    length = smoothed.shape[0]
    grouped = smoothed.reshape(length, decay_map.shape[0], decay_map.shape[1])
    retain = jax.nn.sigmoid(
        jnp.einsum("thi,hio->tho", grouped, decay_map, preferred_element_type=jnp.float32).reshape(
            length, rec_cols
        )
    )
    admit = jax.nn.sigmoid(
        jnp.einsum("thi,hio->tho", grouped, input_map, preferred_element_type=jnp.float32).reshape(
            length, rec_cols
        )
    )
    log_decay = -RATE_SCALE * retain * jax.nn.softplus(-decay_base)[None, :] + decay_jump
    decay = jnp.exp(log_decay)
    inflow = jnp.sqrt(-jnp.expm1(2.0 * log_decay)) * admit * smoothed.astype(jnp.float32)
    products, local_state = lax.associative_scan(chain_step, (decay, inflow), axis=0)
    entering = prefix(
        (products[-1], local_state[-1]),
        "sp",
        chain_step,
        (jnp.ones((rec_cols,), jnp.float32), jnp.zeros((rec_cols,), jnp.float32)),
    )
    state = local_state + products * entering[1][None, :]
    rec_out = (jax.nn.gelu(rec_gate.astype(jnp.float32)) * state).astype(jnp.bfloat16)
    conv_full, rec_full = (
        lax.all_gather(out_conv_w, "sp", axis=1, tiled=True),
        lax.all_gather(out_rec_w, "sp", axis=1, tiled=True),
    )
    return lax.psum_scatter(
        (
            jnp.dot(conv_out, conv_full, preferred_element_type=jnp.float32)
            + jnp.dot(rec_out, rec_full, preferred_element_type=jnp.float32)
        ).astype(jnp.bfloat16),
        "tp",
        scatter_dimension=0,
        tiled=True,
    )


def solution(mesh):
    in_specs = (
        P(("sp", "tp"), None),
        P(),
        P("sp", "tp"),
        P("sp", "tp"),
        P("sp", "tp"),
        P("sp", "tp"),
        P(None, "tp"),
        P("tp"),
        P("tp"),
        P(None, "tp"),
        P("tp", None, None),
        P("tp", None, None),
        P("tp"),
        P("sp", "tp"),
        P("tp", "sp"),
        P("tp", "sp"),
    )
    out_specs = P(("sp", "tp"), None)
    return jax.shard_map(shards, mesh=mesh, in_specs=in_specs, out_specs=out_specs, check_vma=False)
```

profile of v0, /device:TPU:0, one launch (start us, length us, event | category | flops | bytes accessed | tf_op | source)
XLA Modules:
  0.0 595.2 jit_solution(5956597621449933548)
XLA Ops:
  14.3 10.8 %all-gather.10.cloned.1.call-done = bf16[384,4096]{1,0:T(8,128)(2,1)} async-done(((bf16[192,4096]{1,0:T(8,128)(2,1)}), bf16[384,4096]{1,0:T(8,128)(2,1)}) %all-gather.10.cloned.1.call-update) | async-done | bytes 3145744 | tf_op jit(solution)/shard_map/all_gather | solution.py:83
  25.1 79.6 %all-gather.12.cloned.1.call-done = bf16[4096,512]{1,0:T(8,128)(2,1)} async-done(((bf16[256,512]{1,0:T(8,128)(2,1)}), bf16[4096,512]{1,0:T(8,128)(2,1)}) %all-gather.12.cloned.1.call-update) | async-done | bytes 4194320 | tf_op jit(solution)/shard_map/all_gather | solution.py:80
  104.7 4.9 fusion.16
  109.6 72.1 %all-gather.14.cloned.1.call-done = bf16[4096,512]{1,0:T(8,128)(2,1)} async-done(((bf16[256,512]{1,0:T(8,128)(2,1)}), bf16[4096,512]{1,0:T(8,128)(2,1)}) %all-gather.14.cloned.1.call-update) | async-done | bytes 4194320 | tf_op jit(solution)/shard_map/all_gather | solution.py:81
  181.7 5.0 fusion.15
  186.8 3.4 collective-permute-start
  191.9 3.7 fusion.87
  195.6 2.5 psum.14
  198.3 2.5 psum.15
  200.8 75.6 %all-gather.20.cloned.1.call-done = bf16[4096,768]{1,0:T(8,128)(2,1)} async-done(((bf16[256,768]{1,0:T(8,128)(2,1)}), bf16[4096,768]{1,0:T(8,128)(2,1)}) %all-gather.20.cloned.1.call-update) | async-done | bytes 6291472 | tf_op jit(solution)/shard_map/all_gather | solution.py:92
  276.4 6.3 %convolution_convert_fusion = bf16[384,768]{1,0:T(8,128)(2,1)S(1)} fusion(bf16[384,4096]{1,0:T(8,128)(2,1)} %all-gather.10.cloned.1.call-done, bf16[4096,768]{1,0:T(8,128)(2,1)} %all-gather.20.cloned.1.call-done), kind=kOutput, calls=%fused_computation.21 | convolution fusion | flops 2416214016 | bytes 10027008 | tf_op jit(solution)/shard_map/dot_general | solution.py:97
  282.7 3.5 collective-permute-start.1
  295.1 4.4 convert_multiply_fusion.5
  299.5 3.8 slice.533
  309.6 2.8 multiply_add_fusion.2
  312.3 2.6 slice.539
  314.9 2.6 slice.540
  317.5 2.6 slice.538
  320.0 2.6 slice.542
  373.1 2.6 slice.537
  375.7 2.6 slice.588
  381.0 2.2 slice.531
  391.9 2.8 pad.113
  398.5 2.9 pad.112
  402.1 39.9 %all-gather.1 = f32[16,1,768]{2,1,0:T(1,128)S(1)} all-gather(f32[1,1,768]{2,1,0:T(1,128)S(1)} %add_bitcast_fusion), channel_id=1, replica_groups=mesh['sp'=16,'tp'=2] {'sp'}, dimensions={0}, use_global_device_ids=true | all-gather | bytes 52224 | tf_op jit(solution)/shard_map/all_gather | solution.py:20
  442.1 3.0 pad.129
  445.2 2.8 pad.128
  448.7 37.4 %all-gather = f32[16,1,768]{2,1,0:T(1,128)S(1)} all-gather(f32[1,1,768]{2,1,0:T(1,128)S(1)} %add_bitcast_fusion.1), channel_id=1, replica_groups=mesh['sp'=16,'tp'=2] {'sp'}, dimensions={0}, use_global_device_ids=true | all-gather | bytes 52224 | tf_op jit(solution)/shard_map/all_gather | solution.py:20
  486.2 16.1 %fusion.59 = f32[384,4096]{1,0:T(8,128)} fusion(bf16[768,4096]{1,0:T(8,128)(2,1)} %all-gather.22.cloned.1.call-done, bf16[384,4096]{1,0:T(8,128)(2,1)} %all-gather.10.cloned.1.call-done, bf16[4096,768]{1,0:T(8,128)(2,1)} %all-gather.18.cloned.1.call-done, f32[384,768]{1,0:T(8,128)} %pad.128, f32[384,768]{1,0:T(8,128)} %pad.129, f32[384,768]{1,0:T(8,128)} %pad.112, ...), kind=kOutput, calls=%fused_computation.114 | convolution fusion | flops 4836556800 | bytes 26741760 | tf_op jit(solution)/shard_map/dot_general | solution.py:138
  502.2 68.9 %all-gather.16.cloned.1.call-done = bf16[512,4096]{1,0:T(8,128)(2,1)} async-done(((bf16[512,256]{1,0:T(8,128)(2,1)}), bf16[512,4096]{1,0:T(8,128)(2,1)}) %all-gather.16.cloned.1.call-update) | async-done | bytes 4194320 | tf_op jit(solution)/shard_map/all_gather | solution.py:132
  571.1 7.7 %add_convert_fusion = bf16[384,4096]{1,0:T(8,128)(2,1)} fusion(f32[384,4096]{1,0:T(8,128)} %fusion.59, bf16[512,4096]{1,0:T(8,128)(2,1)} %all-gather.16.cloned.1.call-done, f32[384,512]{1,0:T(8,128)S(1)} %get-tuple-element.65, f32[512]{0:T(512)S(1)} %copy-done.22, f32[384]{0:T(512)S(1)} %add_rsqrt_fusion, f32[384]{0:T(512)S(1)} %broadcast_multiply_fusion), kind=kOutput, calls=%fused_computation.3 | convolution fusion | flops 1615331328 | bytes 14423040 | tf_op jit(solution)/shard_map/dot_general | solution.py:137
  578.8 9.5 %reduce-scatter.2.cloned.1.call-done = bf16[192,4096]{1,0:T(8,128)(2,1)} async-done(((bf16[384,4096]{1,0:T(8,128)(2,1)}), bf16[192,4096]{1,0:T(8,128)(2,1)}) %reduce-scatter.2.cloned.1.call-update) | async-done | bytes 1572880 | tf_op jit(solution)/shard_map/reduce_scatter | solution.py:135
  (247 shorter events, 91.4 us)
Async XLA Ops:
  6.5 282.6 %copy-start = (bf16[12,64,64]{2,1,0:T(8,128)(2,1)S(1)}, bf16[12,64,64]{2,1,0:T(8,128)(2,1)}, u32[]{:S(2)}) copy-start(bf16[12,64,64]{2,1,0:T(8,128)(2,1)} %param.28) | copy-start | bytes 294916
  6.5 18.6 %all-gather.10.cloned.1.call-start = ((), (), s32[]{:S(2)}) async-start(), calls=%async_computation.1 | async-start | bytes 4718592 | tf_op jit(solution)/shard_map/all_gather | solution.py:83
  10.1 4.1 copy-start.14
  10.2 4.1 copy-start.38
  10.2 4.1 copy-start.39
  10.2 94.5 %all-gather.12.cloned.1.call-start = ((), (), s32[]{:S(2)}) async-start(), calls=%async_computation.2 | async-start | bytes 4456448 | tf_op jit(solution)/shard_map/all_gather | solution.py:80
  10.9 170.8 %all-gather.14.cloned.1.call-start = ((), (), s32[]{:S(2)}) async-start(), calls=%async_computation.3 | async-start | bytes 4456448 | tf_op jit(solution)/shard_map/all_gather | solution.py:81
  11.7 264.7 %all-gather.20.cloned.1.call-start = ((), (), s32[]{:S(2)}) async-start(), calls=%async_computation.6 | async-start | bytes 6684672 | tf_op jit(solution)/shard_map/all_gather | solution.py:92
  12.2 473.9 %all-gather.18.cloned.1.call-start = ((), (), s32[]{:S(2)}) async-start(), calls=%async_computation.5 | async-start | bytes 6684672 | tf_op jit(solution)/shard_map/all_gather | solution.py:91
  12.8 473.3 %all-gather.22.cloned.1.call-start = ((), (), s32[]{:S(2)}) async-start(), calls=%async_computation.7 | async-start | bytes 6684672 | tf_op jit(solution)/shard_map/all_gather | solution.py:133
  13.4 557.7 %all-gather.16.cloned.1.call-start = ((), (), s32[]{:S(2)}) async-start(), calls=%async_computation.4 | async-start | bytes 4456448 | tf_op jit(solution)/shard_map/all_gather | solution.py:132
  14.2 574.2 %reduce-scatter.2.cloned.1.call-start = ((), (), s32[]{:S(2)}) async-start(), calls=%async_computation.8 | async-start | bytes 4718592 | tf_op jit(solution)/shard_map/reduce_scatter | solution.py:135
  186.8 5.1 copy-start.40
  186.8 4.9 collective-permute-start
  282.7 4.7 collective-permute-start.1
  299.5 3.8 copy-start.2
  381.0 5.6 copy-start.17
  381.0 5.6 copy-start.18
  381.0 5.6 copy-start.19
  381.0 5.6 copy-start.20
  381.0 5.8 copy-start.21
  381.0 5.8 copy-start.34
  381.0 5.8 copy-start.35
  383.2 3.7 copy-start.15
  383.2 3.7 copy-start.16
  383.2 3.8 copy-start.31
  383.2 3.8 copy-start.30
  398.5 43.6 %copy-start.7 = (f32[192,768]{1,0:T(8,128)S(1)}, f32[192,768]{1,0:T(8,128)}, u32[]{:S(2)}) copy-start(f32[192,768]{1,0:T(8,128)} %add.423) | copy-start | bytes 1769476
  401.3 43.8 %copy-start.6 = (f32[191,768]{1,0:T(8,128)S(1)}, f32[191,768]{1,0:T(8,128)}, u32[]{:S(2)}) copy-start(f32[191,768]{1,0:T(8,128)} %get-tuple-element.75) | copy-start | bytes 1760260
  401.3 43.8 %copy-start.36 = (f32[1,768]{1,0:T(1,128)S(1)}, f32[1,768]{1,0:T(1,128)}, u32[]{:S(2)}) copy-start(f32[1,768]{1,0:T(1,128)} %slice.706) | copy-start | bytes 9220
  486.2 85.0 %copy-start.22 = (f32[512]{0:T(512)S(1)}, f32[512]{0:T(512)}, u32[]{:S(2)}) copy-start(f32[512]{0:T(512)} %param.26) | copy-start | bytes 6148
  578.8 9.5 %copy-start.1 = (bf16[12,64,64]{2,1,0:T(8,128)(2,1)S(1)}, bf16[12,64,64]{2,1,0:T(8,128)(2,1)}, u32[]{:S(2)}) copy-start(bf16[12,64,64]{2,1,0:T(8,128)(2,1)} %param.28) | copy-start | bytes 294916
  (20 other events, 27.5 us)
Sparse Core Ops, SparseCore 0:
  10.3 14.8 all-gather.9
  27.9 76.7 all-gather.11
  107.5 74.1 all-gather.13
  184.3 91.9 all-gather.19
  279.0 91.9 all-gather.17
  373.6 109.6 all-gather.21
  486.0 85.0 all-gather.15
  578.9 9.3 reduce-scatter.1
where the time goes:
time: 598 us; the launch traced here: 595 us
  waiting for transfers between devices  323 us (54%)
  local copies, waits for them, and re-layouts  96.5 us (16%)
  blocking collectives  82.3 us (14%)
  matrix products  43.2 us (7%)
  other arithmetic  28.9 us (5%)
  between operations  14.4 us (2%)
  starting transfers between devices  7.15 us (1%)
    all_gather x1, waiting for transfers between devices, shards(): lax.all_gather(conv_val_w, 'sp', axis=0, tiled=True)  79.6 us
    all_gather x2, blocking collectives, prefix(): gathered = jax.tree.map(lambda a: lax.all_gather(a, axis), part)  77.3 us
    slice x56, local copies, waits for them, and re-layouts, shards(): lax.associative_scan(chain_step, (decay, inflow), axis=0)  76.7 us
    all_gather x1, waiting for transfers between devices, shards(): lax.all_gather(rec_in_w, 'sp', axis=0, tiled=True)  75.6 us
    all_gather x1, waiting for transfers between devices, shards(): lax.all_gather(conv_gate_w, 'sp', axis=0, tiled=True)  72.1 us
    all_gather x1, waiting for transfers between devices, shards(): lax.all_gather(out_conv_w, 'sp', axis=1, tiled=True)  68.9 us
    dot_general x1, matrix products, shards(): jnp.dot(rec_out, rec_full, preferred_element_type=jnp.float32)  16.1 us
    pad x30, local copies, waits for them, and re-layouts, shards(): lax.associative_scan(chain_step, (decay, inflow), axis=0)  13.2 us
  transfers between devices with their start and end apart: 10, of which 8 were waited for; matrix products, arithmetic and copies ran while one was open for 26% of the time, Pallas kernels for 0%

commit v1 on v0

--- a/solution.py
+++ b/solution.py
@@ -1,6 +1,10 @@
+import functools
+
 import jax
 import jax.numpy as jnp
 from jax import lax
+from jax.experimental import pallas as pl
+from jax.experimental.pallas import tpu as pltpu
 from jax.sharding import PartitionSpec as P
 
 CONV_WIDTH = 1024
@@ -143,6 +147,469 @@
     )
 
 
+MESH = pl.DeviceIdType.MESH
+ANY = pl.BlockSpec(memory_space=pl.ANY)
+VMEM = pl.BlockSpec(memory_space=pltpu.VMEM)
+SEGMENTS = 8
+
+
+class Spot:
+    def __init__(self, planes):
+        self.s, self.c = lax.axis_index("sp"), lax.axis_index("tp")
+        self.z, self.q = self.s // 4, self.s % 4
+        self.qx = self.q + 1 - 2 * (self.q % 2)
+        self.qy = (self.q + 2) % 4
+        self.qd = 3 - self.q
+        self.has_up, self.has_down = self.z < planes - 1, self.z > 0
+        self.up, self.down = self.at(self.s + 4, self.c), self.at(self.s - 4, self.c)
+        self.partner = self.at(self.s, 1 - self.c)
+
+    def at(self, s, c):
+        return {"sp": s, "tp": c}
+
+    def mate(self, q):
+        return self.at(self.z * 4 + q, self.c)
+
+
+class Mail:
+    def __init__(self, send_sem):
+        self.send_sem, self.count, self.open = send_sem, 0, []
+
+    def send(self, src, dst, recv, device, when=None):
+        copy = pltpu.make_async_remote_copy(
+            src_ref=src, dst_ref=dst, send_sem=self.send_sem.at[self.count],
+            recv_sem=recv, device_id=device, device_id_type=MESH,
+        )
+        self.count += 1
+        self.open.append((copy.wait_send, when))
+        if when is None:
+            copy.start()
+        else:
+            pl.when(when)(copy.start)
+
+    def local(self, src, dst):
+        copy = pltpu.make_async_copy(src, dst, self.send_sem.at[self.count])
+        self.count += 1
+        copy.start()
+        self.open.append((copy.wait, None))
+
+    def arrived(self, dst, recv, device):
+        pltpu.make_async_remote_copy(
+            src_ref=dst, dst_ref=dst, send_sem=self.send_sem.at[0],
+            recv_sem=recv, device_id=device, device_id_type=MESH,
+        ).wait_recv()
+
+    def finish(self):
+        for wait, when in self.open:
+            if when is None:
+                wait()
+            else:
+                pl.when(when)(wait)
+
+
+def greet(me, devices, line):
+    barrier = pltpu.get_barrier_semaphore()
+    for device in devices:
+        pl.semaphore_signal(barrier, inc=1, device_id=device, device_id_type=MESH)
+    amount = len(devices)
+    if line:
+        for has, device in ((me.has_up, me.up), (me.has_down, me.down)):
+            @pl.when(has)
+            def _():
+                pl.semaphore_signal(barrier, inc=1, device_id=device, device_id_type=MESH)
+        amount = amount + me.has_up.astype(jnp.int32) + me.has_down.astype(jnp.int32)
+    pl.semaphore_wait(barrier, amount)
+
+
+class PlaneGather:
+    def __init__(self, me, mail, own, slot, recv, recv_pair):
+        self.me, self.mail, self.own, self.slot = me, mail, own, slot
+        self.recv, self.recv_pair = recv, recv_pair
+
+    def start(self):
+        me, mail = self.me, self.mail
+        for h in (0, 1):
+            for q, half in ((me.qx, h), (me.qy, 1 - h)):
+                mail.send(self.own(half), self.slot(me.q, me.c, half), self.recv.at[me.q, half], me.mate(q))
+        for half in (0, 1):
+            mail.send(self.own(half), self.slot(me.q, me.c, half), self.recv_pair.at[me.q, half], me.partner)
+
+    def took(self, q, half):
+        me, mail = self.me, self.mail
+        here = self.slot(q, me.c, half)
+        mail.arrived(here, self.recv.at[q, half], me.partner)
+        return here
+
+    def share(self, q, half, here):
+        self.mail.send(here, here, self.recv_pair.at[q, half], self.me.partner)
+
+    def first(self):
+        me = self.me
+        for q, half, to in ((me.qx, 0, me.qy), (me.qy, 1, me.qx)):
+            here = self.took(q, half)
+            self.mail.send(here, here, self.recv.at[q, half], me.mate(to))
+            self.share(q, half, here)
+
+    def second(self):
+        for q, half in ((self.me.qx, 1), (self.me.qy, 0)):
+            self.share(q, half, self.took(q, half))
+
+    def third(self):
+        for half in (0, 1):
+            self.share(self.me.qd, half, self.took(self.me.qd, half))
+
+    def last(self):
+        me = self.me
+        for q in (me.q, me.qx, me.qy, me.qd):
+            for half in (0, 1):
+                self.mail.arrived(self.slot(q, 1 - me.c, half), self.recv_pair.at[q, half], me.partner)
+
+
+def enter_kernel(planes, x_ref, w_ref, j_ref, xall, wall, jall, send, rx, rp, rw, rz, rj):
+    me = Spot(planes)
+    mail = Mail(send)
+    greet(me, [me.mate(me.qx), me.mate(me.qy), me.mate(me.qd), me.partner], True)
+    others = (me.qx, me.qy, me.qd)
+
+    def to_line(src, origin, piece):
+        index = origin * 4 + piece
+        mail.send(src, wall.at[index], rz.at[origin, piece], me.up, me.has_up)
+        mail.send(src, wall.at[index], rz.at[origin, piece], me.down, me.has_down)
+
+    for q in others:
+        mail.send(w_ref.at[q], wall.at[me.s], rw.at[me.q], me.mate(q))
+    to_line(w_ref.at[me.q], me.z, me.q)
+    half_rows = x_ref.shape[0] // 2
+    xg = PlaneGather(
+        me, mail,
+        lambda h: x_ref.at[pl.ds(h * half_rows, half_rows)],
+        lambda q, c, h: xall.at[q * 2 + c, pl.ds(h * half_rows, half_rows)],
+        rx, rp,
+    )
+    xg.start()
+    for q in others:
+        mail.send(j_ref.at[q], jall.at[me.q], rj.at[me.q], me.mate(q))
+    mail.local(x_ref, xall.at[me.q * 2 + me.c])
+    mail.local(w_ref.at[me.q], wall.at[me.s])
+    mail.local(j_ref.at[me.q], jall.at[me.q])
+    for q in others:
+        here = wall.at[me.z * 4 + q]
+        mail.arrived(here, rw.at[q], me.partner)
+        to_line(here, me.z, q)
+
+    def line_step(k):
+        for piece in (me.q,) + others:
+            for origin, there, on, more in (
+                (me.z - k, me.z >= k, me.up, me.has_up),
+                (me.z + k, me.z + k < planes, me.down, me.has_down),
+            ):
+                here = wall.at[origin * 4 + piece]
+                sem = rz.at[origin, piece]
+                pl.when(there)(functools.partial(mail.arrived, here, sem, me.partner))
+                if k < planes - 1:
+                    mail.send(here, here, sem, on, jnp.logical_and(there, more))
+
+    line_step(1)
+    xg.first()
+    for k in range(2, planes - 1):
+        line_step(k)
+    xg.second()
+    for q in others:
+        mail.arrived(jall.at[q], rj.at[q], me.partner)
+    xg.third()
+    line_step(planes - 1)
+    xg.last()
+    mail.finish()
+
+
+def enter(planes, normed, pieces, jumps):
+    rows, width = normed.shape
+    dma = pltpu.SemaphoreType.DMA
+    return pl.pallas_call(
+        functools.partial(enter_kernel, planes),
+        out_shape=(
+            jax.ShapeDtypeStruct((8, rows, width), normed.dtype),
+            jax.ShapeDtypeStruct((planes * 4,) + pieces.shape[1:], pieces.dtype),
+            jax.ShapeDtypeStruct(jumps.shape, jumps.dtype),
+        ),
+        in_specs=[VMEM] * 3,
+        out_specs=(ANY,) * 3,
+        scratch_shapes=[dma((40 + 8 * planes,)), dma((4, 2)), dma((4, 2)), dma((4,)), dma((planes, 4)), dma((4,))],
+        compiler_params=pltpu.CompilerParams(collective_id=0, has_side_effects=True),
+    )(normed, pieces, jumps)
+
+
+def small_kernel(planes, st_ref, cr_ref, st_all, cr_all, send, rs, rc):
+    me = Spot(planes)
+    mail = Mail(send)
+    mine = me.q * 2 + me.c
+    mates = [me.at(me.z * 4 + (me.q + dq) % 4, c) for dq in range(4) for c in (me.c, 1 - me.c)][1:]
+    lined = [me.at((me.s + 4 * k) % (4 * planes), me.c) for k in range(1, planes)]
+    greet(me, mates + lined, False)
+    for device in lined:
+        mail.send(cr_ref, cr_all.at[me.z], rc.at[me.z], device)
+    for device in mates:
+        mail.send(st_ref, st_all.at[mine], rs.at[mine], device)
+    mail.local(st_ref, st_all.at[mine])
+    mail.local(cr_ref, cr_all.at[me.z])
+    for k in range(1, planes):
+        z = (me.z + k) % planes
+        mail.arrived(cr_all.at[z], rc.at[z], me.partner)
+    for k in range(1, 8):
+        d = (mine + k) % 8
+        mail.arrived(st_all.at[d], rs.at[d], me.partner)
+    mail.finish()
+
+
+def small(planes, stats, carry):
+    dma = pltpu.SemaphoreType.DMA
+    return pl.pallas_call(
+        functools.partial(small_kernel, planes),
+        out_shape=(
+            jax.ShapeDtypeStruct((8,) + stats.shape, stats.dtype),
+            jax.ShapeDtypeStruct((planes,) + carry.shape, carry.dtype),
+        ),
+        in_specs=[ANY] * 2,
+        out_specs=(ANY,) * 2,
+        scratch_shapes=[dma((12 + planes,)), dma((8,)), dma((planes,))],
+        compiler_params=pltpu.CompilerParams(collective_id=1, has_side_effects=True),
+    )(stats, carry)
+
+
+def middle_kernel(planes, y_ref, w_ref, yall, wz, wp, send, ry, rp, rz, rw):
+    me = Spot(planes)
+    mail = Mail(send)
+    greet(me, [me.mate(me.qx), me.mate(me.qy), me.mate(me.qd), me.partner], True)
+    half_rows, width = y_ref.shape[0] // 2, y_ref.shape[1]
+    part = planes // 2
+
+    def hand_over(src, origin, when):
+        theirs = origin // part != me.c
+        if when is not None:
+            theirs = jnp.logical_and(theirs, when)
+        place = origin - (1 - me.c) * part
+        mail.send(src, wp.at[place], rw.at[place], me.partner, theirs)
+
+    yg = PlaneGather(
+        me, mail,
+        lambda h: y_ref.at[pl.ds(h * half_rows, half_rows)],
+        lambda q, c, h: yall.at[
+            pl.ds(h * half_rows, half_rows), pl.ds(pl.multiple_of((q * 2 + c) * width, 128), width)
+        ],
+        ry, rp,
+    )
+    mail.send(w_ref, wz.at[me.z], rz.at[me.z], me.up, me.has_up)
+    mail.send(w_ref, wz.at[me.z], rz.at[me.z], me.down, me.has_down)
+    yg.start()
+    hand_over(w_ref, me.z, None)
+    mail.local(w_ref, wz.at[me.z])
+    mail.local(y_ref, yall.at[:, pl.ds(pl.multiple_of((me.q * 2 + me.c) * width, 128), width)])
+
+    def line_step(k):
+        for origin, there, on, more in (
+            (me.z - k, me.z >= k, me.up, me.has_up),
+            (me.z + k, me.z + k < planes, me.down, me.has_down),
+        ):
+            pl.when(there)(functools.partial(mail.arrived, wz.at[origin], rz.at[origin], me.partner))
+            if k < planes - 1:
+                mail.send(wz.at[origin], wz.at[origin], rz.at[origin], on, jnp.logical_and(there, more))
+            hand_over(wz.at[origin], origin, there)
+
+    yg.first()
+    line_step(1)
+    yg.second()
+    for k in range(2, planes):
+        if k == planes - 1:
+            yg.third()
+        line_step(k)
+    yg.last()
+    for k in range(part):
+        mail.arrived(wp.at[k], rw.at[k], me.partner)
+    mail.finish()
+
+
+def middle(planes, mine, weights):
+    rows, width = mine.shape
+    dma = pltpu.SemaphoreType.DMA
+    return pl.pallas_call(
+        functools.partial(middle_kernel, planes),
+        out_shape=(
+            jax.ShapeDtypeStruct((rows, 8 * width), mine.dtype),
+            jax.ShapeDtypeStruct((planes,) + weights.shape, weights.dtype),
+            jax.ShapeDtypeStruct((planes // 2,) + weights.shape, weights.dtype),
+        ),
+        in_specs=[VMEM] * 2,
+        out_specs=(ANY,) * 3,
+        scratch_shapes=[dma((24 + 5 * planes,)), dma((4, 2)), dma((4, 2)), dma((planes,)), dma((planes // 2,))],
+        compiler_params=pltpu.CompilerParams(collective_id=2, has_side_effects=True),
+    )(mine, weights)
+
+
+def leave_kernel(planes, c_ref, out, send, recv):
+    me = Spot(planes)
+    mail = Mail(send)
+    mine = me.q * 2 + me.c
+    mates = [((me.q + dq) % 4, c) for dq in (3, 1, 2, 0) for c in (me.c, 1 - me.c)]
+    mates = [(q, c) for i, (q, c) in enumerate(mates) if i != 6]
+    devices = [me.at(me.z * 4 + q, c) for q, c in mates]
+    greet(me, devices, False)
+    for (q, c), device in zip(mates, devices):
+        mail.send(c_ref.at[q * 2 + c], out.at[mine], recv.at[mine], device)
+    mail.local(c_ref.at[mine], out.at[mine])
+    for q, c in mates:
+        mail.arrived(out.at[q * 2 + c], recv.at[q * 2 + c], me.partner)
+    mail.finish()
+
+
+def leave(planes, blocks):
+    dma = pltpu.SemaphoreType.DMA
+    return pl.pallas_call(
+        functools.partial(leave_kernel, planes),
+        out_shape=jax.ShapeDtypeStruct(blocks.shape, blocks.dtype),
+        in_specs=[VMEM],
+        out_specs=ANY,
+        scratch_shapes=[dma((8,)), dma((8,))],
+        compiler_params=pltpu.CompilerParams(collective_id=3, has_side_effects=True),
+    )(blocks)
+
+
+def scan_kernel(d_ref, u_ref, p_ref, s_ref):
+    def one(i, held):
+        product, state = held
+        decay = d_ref[i]
+        product, state = product * decay, state * decay + u_ref[i]
+        p_ref[i] = product
+        s_ref[i] = state
+        return product, state
+
+    shape = d_ref.shape[1:]
+    lax.fori_loop(
+        0, d_ref.shape[0], one, (jnp.ones(shape, jnp.float32), jnp.zeros(shape, jnp.float32)), unroll=8
+    )
+
+
+def plane_shards(
+    planes,
+    tokens,
+    norm_gain,
+    conv_val_w,
+    conv_gate_w,
+    rec_gate_w,
+    rec_in_w,
+    conv_taps,
+    conv_bias,
+    conv_gain,
+    short_taps,
+    decay_map,
+    input_map,
+    decay_base,
+    decay_jump,
+    out_conv_w,
+    out_rec_w,
+):
+    s, c = lax.axis_index("sp"), lax.axis_index("tp")
+    z, q = s // 4, s % 4
+    f32, bf16 = jnp.float32, jnp.bfloat16
+
+    def by_mate(a):
+        return a.reshape(a.shape[0], 4, a.shape[1] // 4).transpose(1, 0, 2)
+
+    def mine(a, axis):
+        size = a.shape[axis] // 4
+        return lax.dynamic_slice_in_dim(a, q * size, size, axis)
+
+    normed = norm_rows(tokens, norm_gain)
+    pieces = jnp.concatenate([by_mate(w) for w in (conv_val_w, conv_gate_w, rec_gate_w, rec_in_w)], axis=2)
+    xall, wall, jall = enter(planes, normed, pieces, by_mate(decay_jump))
+    length = xall.shape[0] * xall.shape[1]
+    cw, rw = conv_val_w.shape[1] // 4, rec_in_w.shape[1] // 4
+    xall = xall.reshape(length, xall.shape[2])
+    wall = wall.reshape(-1, wall.shape[2])
+    jump = jall.reshape(length, rw)
+    projected = jnp.dot(xall, wall, preferred_element_type=f32).astype(bf16)
+    glu = glu_of(projected[:, :cw], projected[:, cw : 2 * cw])
+    rec_gate, rec_in = projected[:, 2 * cw : 2 * cw + rw], projected[:, 2 * cw + rw :]
+    conv_lags, short_lags = conv_taps.shape[0] - 1, short_taps.shape[0] - 1
+    edge = passed_along(jnp.concatenate([glu[-conv_lags:], rec_in[-conv_lags:]], axis=1), "sp", 4)
+
+    filtered = causal_window(edge[:, :cw], glu, mine(conv_taps, 1)) + mine(conv_bias, 0)[None, :]
+    local_sum = jnp.sum(filtered, axis=1)
+    off = filtered - (local_sum / cw)[:, None]
+    local_spread = jnp.sum(off * off, axis=1)
+    stats = jnp.stack([local_sum, local_spread]).reshape(-1, 128)
+
+    smoothed = causal_window(edge[-short_lags:, cw:], rec_in, mine(short_taps, 1)).astype(bf16)
+    heads, size = decay_map.shape[0] // 4, decay_map.shape[1]
+    eye = jnp.eye(heads, dtype=bf16)
+
+    def widened(m):
+        return (mine(m, 0)[:, :, None, :] * eye[:, None, :, None]).reshape(rw, rw)
+
+    gates = jax.nn.sigmoid(
+        jnp.dot(
+            smoothed,
+            jnp.concatenate([widened(decay_map), widened(input_map)], axis=1),
+            preferred_element_type=f32,
+        )
+    )
+    retain, admit = gates[:, :rw], gates[:, rw:]
+    log_decay = -RATE_SCALE * retain * jax.nn.softplus(-mine(decay_base, 0))[None, :] + jump
+    decay = jnp.exp(log_decay)
+    inflow = jnp.sqrt(-jnp.expm1(2.0 * log_decay)) * admit * smoothed.astype(f32)
+    steps = length // SEGMENTS
+
+    def by_step(a):
+        return a.reshape(SEGMENTS, steps, rw).transpose(1, 0, 2)
+
+    products, states = pl.pallas_call(
+        scan_kernel,
+        out_shape=(jax.ShapeDtypeStruct((steps, SEGMENTS, rw), f32),) * 2,
+        in_specs=[VMEM] * 2,
+        out_specs=(VMEM,) * 2,
+    )(by_step(decay), by_step(inflow))
+    seg_p, seg_s = products[-1], states[-1]
+    total = (jnp.ones((rw,), f32), jnp.zeros((rw,), f32))
+    for i in range(SEGMENTS):
+        total = chain_step(total, (seg_p[i], seg_s[i]))
+    st_all, cr_all = small(planes, stats, jnp.stack(total))
+
+    st_all = st_all.reshape(8, 2, length)
+    width = 8 * cw
+    mean = jnp.sum(st_all[:, 0], axis=0) / width
+    shift = st_all[:, 0] / cw - mean[None]
+    spread = jnp.sum(st_all[:, 1] + cw * shift * shift, axis=0) / width
+    conv_out = jax.nn.silu(
+        (filtered - mean[:, None]) * lax.rsqrt(spread + 1e-05)[:, None] * mine(conv_gain, 0)[None, :]
+    ).astype(bf16)
+
+    held = jnp.zeros((rw,), f32)
+    for i in range(planes - 1):
+        held = jnp.where(i < z, cr_all[i, 0] * held + cr_all[i, 1], held)
+    entering = []
+    for i in range(SEGMENTS):
+        entering.append(held)
+        held = seg_p[i] * held + seg_s[i]
+    state = (states + products * jnp.stack(entering)[None]).transpose(1, 0, 2).reshape(length, rw)
+    rec_out = (jax.nn.gelu(rec_gate.astype(f32)) * state).astype(bf16)
+    fill = -(cw + rw) % 128
+    block = jnp.concatenate([conv_out, rec_out, jnp.zeros((length, fill), bf16)], axis=1)
+
+    cols = out_conv_w.shape[1]
+    rows_by_mate = jnp.concatenate(
+        [out_conv_w.reshape(4, cw, cols), out_rec_w.reshape(4, rw, cols)], axis=1
+    ).reshape(-1, cols)
+    yall, wz, wp = middle(planes, block, rows_by_mate)
+    part = planes // 2
+    own = lax.dynamic_slice_in_dim(wz, c * part, part, 0)
+    both = jnp.stack([jnp.where(c == 0, own, wp), jnp.where(c == 0, wp, own)])
+    both = both.reshape(2, part, 4, cw + rw, cols).transpose(2, 0, 3, 1, 4)
+    both = jnp.pad(both, ((0, 0), (0, 0), (0, fill), (0, 0), (0, 0))).reshape(-1, part * cols)
+    mixed = jnp.dot(yall, both, preferred_element_type=f32).astype(bf16)
+    out = leave(planes, mixed.reshape(8, length // 8, part * cols))
+    out = out.reshape(4, 2, length // 8, part, cols).transpose(2, 1, 3, 0, 4)
+    return out.reshape(length // 8, -1)
+
+
 def solution(mesh):
     in_specs = (
         P(("sp", "tp"), None),
@@ -163,4 +630,7 @@
         P("tp", "sp"),
     )
     out_specs = P(("sp", "tp"), None)
-    return jax.shard_map(shards, mesh=mesh, in_specs=in_specs, out_specs=out_specs, check_vma=False)
+    count = mesh.shape["sp"]
+    planar = mesh.shape["tp"] == 2 and count % 8 == 0
+    body = functools.partial(plane_shards, count // 4) if planar else shards
+    return jax.shard_map(body, mesh=mesh, in_specs=in_specs, out_specs=out_specs, check_vma=False)

time: 598 us -> 268 us (0.45)
  waiting for transfers between devices: 323 us -> 0.01 us
  Pallas kernels: 0 us -> 178 us
  blocking collectives: 82.3 us -> 0 us
  local copies, waits for them, and re-layouts: 96.5 us -> 32.9 us
  matrix products: 43.2 us -> 21.9 us
  between operations: 14.4 us -> 0.56 us
    all_gather x7 -> x0, waiting for transfers between devices: 307 us -> none  [the longest x1 79.6 us: shards(): lax.all_gather(conv_val_w, 'sp', axis=0, tiled=True)]
    pallas_call x0 -> x5, Pallas kernels: none -> 178 us  [the longest x1 94.4 us: enter(): pl.pallas_call(functools.partial(enter_kernel, planes), out_shape=(jax.Sh...]
    all_gather x2 -> x0, blocking collectives: 77.3 us -> none  [prefix(): gathered = jax.tree.map(lambda a: lax.all_gather(a, axis), part)]
    slice x58 -> x5, local copies, waits for them, and re-layouts: 76.7 us -> 1.84 us  [the longest x1 0.72 us: plane_shards(): edge[-short_lags:, cw:]]
    dot_general x7 -> x3, matrix products: 43.2 us -> 21.9 us  [the longest x1 14.4 us: plane_shards(): projected = jnp.dot(xall, wall, preferred_element_type=f32).astype(bf16)]
    reshape x0 -> x11, local copies, waits for them, and re-layouts: none -> 14.2 us  [the longest x2 4.13 us: by_step(): return a.reshape(SEGMENTS, steps, rw).transpose(1, 0, 2)]
    add x15 -> x1, other arithmetic: 12.4 us -> 1.02 us  [chain_step(): return (earlier[0] * latter[0], latter[0] * earlier[1] + latter[1])]
    pad x30 -> x1, local copies, waits for them, and re-layouts: 13.2 us -> 2.58 us  [plane_shards(): jnp.pad(both, ((0, 0), (0, 0), (0, fill), (0, 0), (0, 0)))]
  transfers between devices with their start and end apart: 10 -> 1, of which waited for: 8 -> 0; matrix products, arithmetic and copies ran while one was open for 26% -> 4% of each run, Pallas kernels for 0% -> 0%
where the time goes in v1:
time: 268 us; the launch traced here: 267 us
  Pallas kernels  178 us (66%)
  local copies, waits for them, and re-layouts  32.9 us (12%)
  other arithmetic  31.1 us (12%)
  matrix products  21.9 us (8%)
  starting transfers between devices  2.85 us (1%)
    pallas_call x1, Pallas kernels, enter(): pl.pallas_call(functools.partial(enter_kernel, planes), out_shape=(jax.Sh...  94.4 us
    pallas_call x1, Pallas kernels, middle(): pl.pallas_call(functools.partial(middle_kernel, planes), out_shape=(jax.S...  51.1 us
    pallas_call x1, Pallas kernels, leave(): pl.pallas_call(functools.partial(leave_kernel, planes), out_shape=jax.Sha...  22.1 us
    dot_general x1, matrix products, plane_shards(): projected = jnp.dot(xall, wall, preferred_element_type=f32).astype(bf16)  14.4 us
    dot_general x1, matrix products, plane_shards(): mixed = jnp.dot(yall, both, preferred_element_type=f32).astype(bf16)  6.36 us
    pallas_call x1, Pallas kernels, small(): pl.pallas_call(functools.partial(small_kernel, planes), out_shape=(jax.Sh...  6.28 us
  transfers between devices with their start and end apart: 1, of which 0 were waited for; matrix products, arithmetic and copies ran while one was open for 4% of the time, Pallas kernels for 0%

profile of v1, /device:TPU:0, one launch (start us, length us, event | category | flops | bytes accessed | tf_op | source)
XLA Modules:
  0.0 267.3 jit_solution(9463131017922353480)
XLA Ops:
  0.0 1.9 fusion
  3.1 1.0 copy.28
  5.8 1.6 copy.32
  7.4 2.3 fusion.2.x_ref
  9.7 1.4 pad_maximum_fusion.w_ref
  11.2 94.4 %shard_map.154 = (bf16[8,192,4096]{2,1,0:T(8,128)(2,1)}, bf16[16,256,640]{2,1,0:T(8,128)(2,1)}, f32[4,384,192]{2,1,0:T(8,128)}) custom-call(bf16[192,4096]{1,0:T(8,128)(2,1)} %fusion.2.x_ref, bf16[4,256,640]{2,1,0:T(8,128)(2,1)} %pad_maximum_fusion.w_ref, f32[4,384,192]{2,1,0:T(8,128)} %bitcast.278), custom_call_target="tpu_custom_call" | custom-call | tf_op jit(solution)/shard_map/pallas_call | solution.py:328
  105.6 14.4 %convolution_convert_fusion = bf16[1536,640]{1,0:T(8,128)(2,1)S(1)} fusion(bf16[1536,4096]{1,0:T(8,128)(2,1)} %bitcast.305, bf16[4096,640]{1,0:T(8,128)(2,1)} %bitcast.308), kind=kOutput, calls=%fused_computation.2 | convolution fusion | flops 8054046720 | bytes 19791872 | tf_op jit(solution)/shard_map/dot_general | solution.py:529
  120.9 2.9 %collective-permute-start = (bf16[30,320]{1,0:T(8,128)(2,1)}, bf16[30,320]{1,0:T(8,128)(2,1)}, u32[]{:S(2)}, u32[]{:S(2)}) collective-permute-start(bf16[30,320]{1,0:T(8,128)(2,1)} %pad_maximum_fusion.2), channel_id=1, source_target_pairs={{0,8},{2,10},{4,12},{6,14},{8,16},{10,18},{12,20},{14,22},{16,24},... | collective-permute-start | bytes 57608 | tf_op jit(solution)/shard_map/ppermute | solution.py:19
  131.9 1.3 dynamic_slice.25
  133.2 1.3 dynamic_slice.30
  135.4 4.1 %fusion.69 = (f32[1536]{0:T(1024)S(1)}, f32[1536,128]{1,0:T(8,128)S(1)}) fusion(f32[128]{0:T(128)} %dynamic_slice.25, f32[1566,128]{1,0:T(8,128)S(1)} %maximum_convert_fusion.1, f32[128]{0:T(128)} %get-tuple-element.43, f32[128]{0:T(128)} %get-tuple-element.44, f32[128]{0:T(128)} %get-tuple-element.45, f32[128]{0:T(128)} %get-tuple-element.46, ...), kind=kLoop, calls=%fused_computation.215 | loop fusion | flops 12384768 | bytes 25188352 | tf_op jit(solution)/shard_map/reduce_sum | solution.py:536
  140.5 1.2 fusion.5
  141.9 1.9 fusion.13
  143.9 2.1 copy.57
  145.9 2.1 copy.56
  149.2 4.0 %shard_map.155 = (f32[192,8,192]{2,1,0:T(8,128)}, f32[192,8,192]{2,1,0:T(8,128)}) custom-call(f32[192,8,192]{2,1,0:T(8,128)} %bitcast.275, f32[192,8,192]{2,1,0:T(8,128)} %bitcast.276), custom_call_target="tpu_custom_call" | custom-call | tf_op jit(solution)/shard_map/pallas_call | solution.py:564
  154.1 1.0 bitcast_add_fusion.2
  155.7 6.3 %shard_map.156 = (f32[8,24,128]{2,1,0:T(8,128)}, f32[4,2,192]{2,1,0:T(2,128)}) custom-call(f32[24,128]{1,0:T(8,128)} %reshape.939.st_ref, f32[2,192]{1,0:T(2,128)} %pad_maximum_fusion.4.cr_ref), custom_call_target="tpu_custom_call" | custom-call | tf_op jit(solution)/shard_map/pallas_call | solution.py:366
  162.0 1.0 bitcast_add_fusion.3
  163.1 2.1 add_bitcast_fusion
  167.9 1.3 maximum_maximum_fusion.y_ref
  169.2 51.1 %shard_map.157 = (bf16[1536,3072]{1,0:T(8,128)(2,1)}, bf16[4,1280,256]{2,1,0:T(8,128)(2,1)}, bf16[2,1280,256]{2,1,0:T(8,128)(2,1)}) custom-call(bf16[1536,384]{1,0:T(8,128)(2,1)} %maximum_maximum_fusion.y_ref, bf16[1280,256]{1,0:T(8,128)(2,1)} %bitcast.285), custom_call_target="tpu_custom_call" | custom-call | tf_op jit(solution)/shard_map/pallas_call | solution.py:434
  220.3 1.9 broadcast_select_fusion.1
  222.2 1.4 copy.39
  223.6 1.4 copy.38
  225.0 3.7 %maximum_bitcast_fusion = bf16[4,2,320,2,256]{4,3,2,1,0:T(2,128)(2,1)S(1)} fusion(bf16[1,2,4,320,256]{4,1,3,0,2:T(2,128)(2,1)S(1)} %copy.39, bf16[1,2,4,320,256]{4,1,3,0,2:T(2,128)(2,1)S(1)} %copy.38), kind=kLoop, calls=%fused_computation.15 | loop fusion | flops 1310720 | bytes 5242880 | tf_op jit(solution)/shard_map/transpose | solution.py:605
  228.7 2.6 pad.4
  232.0 6.4 %convolution_convert_fusion.1 = bf16[1536,512]{1,0:T(8,128)(2,1)} fusion(bf16[1536,3072]{1,0:T(8,128)(2,1)S(1)} %bitcast.307, bf16[3072,512]{1,0:T(8,128)(2,1)S(1)} %bitcast.284), kind=kOutput, calls=%fused_computation.9 | convolution fusion | flops 4832624640 | bytes 14155776 | tf_op jit(solution)/shard_map/dot_general | solution.py:607
  238.4 22.1 %shard_map.158 = bf16[8,192,512]{2,1,0:T(8,128)(2,1)} custom-call(bf16[8,192,512]{2,1,0:T(8,128)(2,1)} %bitcast.288), custom_call_target="tpu_custom_call" | custom-call | tf_op jit(solution)/shard_map/pallas_call | solution.py:466
  260.5 2.4 reshape.950
  262.9 2.0 copy.40
  264.9 2.4 reshape.951
  (92 shorter events, 19.9 us)
Async XLA Ops:
  0.0 2.5 copy-start.5
  0.0 2.9 %copy-start.6 = (bf16[256,768]{1,0:T(8,128)(2,1)S(1)}, bf16[256,768]{1,0:T(8,128)(2,1)}, u32[]{:S(2)}) copy-start(bf16[256,768]{1,0:T(8,128)(2,1)} %param.20) | copy-start | bytes 1179652
  2.5 1.6 copy-start.9
  2.9 1.5 copy-start.10
  3.0 2.3 copy-start.3
  5.7 1.6 copy-start
  5.8 1.6 copy-start.13
  7.4 2.4 copy-start.1
  7.4 2.4 copy-start.4
  120.0 7.2 %copy-start.7 = (bf16[768,256]{1,0:T(8,128)(2,1)S(1)}, bf16[768,256]{1,0:T(8,128)(2,1)}, u32[]{:S(2)}) copy-start(bf16[768,256]{1,0:T(8,128)(2,1)} %param.31) | copy-start | bytes 1179652
  120.0 7.2 %copy-start.8 = (bf16[512,256]{1,0:T(8,128)(2,1)S(1)}, bf16[512,256]{1,0:T(8,128)(2,1)}, u32[]{:S(2)}) copy-start(bf16[512,256]{1,0:T(8,128)(2,1)} %param.30) | copy-start | bytes 786436
  120.9 13.7 %collective-permute-start = (bf16[30,320]{1,0:T(8,128)(2,1)}, bf16[30,320]{1,0:T(8,128)(2,1)}, u32[]{:S(2)}, u32[]{:S(2)}) collective-permute-start(bf16[30,320]{1,0:T(8,128)(2,1)} %pad_maximum_fusion.2), channel_id=1, source_target_pairs={{0,8},{2,10},{4,12},{6,14},{8,16},{10,18},{12,20},{14,22},{16,24},... | collective-permute-start | bytes 57608 | tf_op jit(solution)/shard_map/ppermute | solution.py:19
  139.5 1.0 copy-start.11
  139.5 1.0 copy-start.12
  139.5 1.0 copy-start.14
  139.5 1.0 copy-start.15
  140.5 1.4 copy-start.2
  165.7 1.7 copy-start.16
  223.6 8.4 %slice-start = ((s8[9437184]{0:T(1024)(128)(4,1)}), s8[4194304]{0:T(1024)(128)(4,1)S(1)}, s32[]{:S(2)}) async-start(s8[9437184]{0:T(1024)(128)(4,1)} %bitcast.306), calls=%async_computation | async-start | bytes 8388608
  225.0 7.0 %slice-start.1 = ((s8[9437184]{0:T(1024)(128)(4,1)}), s8[4194304]{0:T(1024)(128)(4,1)S(1)}, s32[]{:S(2)}) async-start(s8[9437184]{0:T(1024)(128)(4,1)} %bitcast.306), calls=%async_computation.1 | async-start | bytes 8388608
  228.7 3.3 %slice-start.2 = ((s8[9437184]{0:T(1024)(128)(4,1)}), s8[1048576]{0:T(1024)(128)(4,1)S(1)}, s32[]{:S(2)}) async-start(s8[9437184]{0:T(1024)(128)(4,1)} %bitcast.306), calls=%async_computation.2 | async-start | bytes 2097152

commit v2 on v1

--- a/solution.py
+++ b/solution.py
@@ -339,49 +339,38 @@
     )(normed, pieces, jumps)
 
 
-def small_kernel(planes, st_ref, cr_ref, st_all, cr_all, send, rs, rc):
+def minus_expm1(y):
+    series = 1.0 + y * (1.0 / 8.0)
+    for n in (7.0, 6.0, 5.0, 4.0, 3.0, 2.0):
+        series = 1.0 + y * (1.0 / n) * series
+    return jnp.where(y > -0.35, -y * series, 1.0 - jnp.exp(y))
+
+
+def gelu(v):
+    return 0.5 * v * (1.0 + jnp.tanh(0.7978845608028654 * (v + 0.044715 * v * v * v)))
+
+
+def core_kernel(
+    planes, lags, proj, jump, cpar, rpar, dmap, imap, w_ref,
+    out, wz, wp, yall, halo, gext, rext, filt, dec, inf, maps, stat, st_all, carry, cr_all,
+    send, ry, rp, rz, rw, rh, rs, rc,
+):
     me = Spot(planes)
     mail = Mail(send)
+    c_lags, s_lags = lags
+    f32, bf16 = jnp.float32, jnp.bfloat16
+    length = proj.shape[0]
+    cw = gext.shape[1]
+    rwid = jump.shape[1]
+    seg = length // SEGMENTS
+    top = halo.shape[0]
+    fold = dec.shape[0]
+    part = planes // 2
+    width = yall.shape[1] // 8
     mine = me.q * 2 + me.c
     mates = [me.at(me.z * 4 + (me.q + dq) % 4, c) for dq in range(4) for c in (me.c, 1 - me.c)][1:]
     lined = [me.at((me.s + 4 * k) % (4 * planes), me.c) for k in range(1, planes)]
     greet(me, mates + lined, False)
-    for device in lined:
-        mail.send(cr_ref, cr_all.at[me.z], rc.at[me.z], device)
-    for device in mates:
-        mail.send(st_ref, st_all.at[mine], rs.at[mine], device)
-    mail.local(st_ref, st_all.at[mine])
-    mail.local(cr_ref, cr_all.at[me.z])
-    for k in range(1, planes):
-        z = (me.z + k) % planes
-        mail.arrived(cr_all.at[z], rc.at[z], me.partner)
-    for k in range(1, 8):
-        d = (mine + k) % 8
-        mail.arrived(st_all.at[d], rs.at[d], me.partner)
-    mail.finish()
-
-
-def small(planes, stats, carry):
-    dma = pltpu.SemaphoreType.DMA
-    return pl.pallas_call(
-        functools.partial(small_kernel, planes),
-        out_shape=(
-            jax.ShapeDtypeStruct((8,) + stats.shape, stats.dtype),
-            jax.ShapeDtypeStruct((planes,) + carry.shape, carry.dtype),
-        ),
-        in_specs=[ANY] * 2,
-        out_specs=(ANY,) * 2,
-        scratch_shapes=[dma((12 + planes,)), dma((8,)), dma((planes,))],
-        compiler_params=pltpu.CompilerParams(collective_id=1, has_side_effects=True),
-    )(stats, carry)
-
-
-def middle_kernel(planes, y_ref, w_ref, yall, wz, wp, send, ry, rp, rz, rw):
-    me = Spot(planes)
-    mail = Mail(send)
-    greet(me, [me.mate(me.qx), me.mate(me.qy), me.mate(me.qd), me.partner], True)
-    half_rows, width = y_ref.shape[0] // 2, y_ref.shape[1]
-    part = planes // 2
 
     def hand_over(src, origin, when):
         theirs = origin // part != me.c
@@ -390,20 +379,106 @@
         place = origin - (1 - me.c) * part
         mail.send(src, wp.at[place], rw.at[place], me.partner, theirs)
 
-    yg = PlaneGather(
-        me, mail,
-        lambda h: y_ref.at[pl.ds(h * half_rows, half_rows)],
-        lambda q, c, h: yall.at[
-            pl.ds(h * half_rows, half_rows), pl.ds(pl.multiple_of((q * 2 + c) * width, 128), width)
-        ],
-        ry, rp,
-    )
+    mail.send(proj.at[pl.ds(length - top, top)], halo, rh.at[0], me.up, me.has_up)
     mail.send(w_ref, wz.at[me.z], rz.at[me.z], me.up, me.has_up)
     mail.send(w_ref, wz.at[me.z], rz.at[me.z], me.down, me.has_down)
-    yg.start()
     hand_over(w_ref, me.z, None)
     mail.local(w_ref, wz.at[me.z])
-    mail.local(y_ref, yall.at[:, pl.ds(pl.multiple_of((me.q * 2 + me.c) * width, 128), width)])
+
+    maps[...] = jnp.zeros_like(maps)
+    size = dmap.shape[1]
+    heads = rwid // size
+    for h in range(heads):
+        spot = pl.ds(h * size, size)
+        maps[spot, pl.ds(h * size, size)] = dmap[me.q * heads + h]
+        maps[spot, pl.ds(fold * 128 + h * size, size)] = imap[me.q * heads + h]
+
+    def columns(ref, row, count):
+        val = ref[pl.ds(row, count), pl.ds(0, cw)].astype(f32)
+        gate = ref[pl.ds(row, count), pl.ds(cw, cw)].astype(f32)
+        return (val * jax.nn.sigmoid(gate)).astype(bf16).astype(f32)
+
+    rec_at, gate_at = 2 * cw + rwid, 2 * cw
+
+    @pl.loop(0, SEGMENTS)
+    def _(i):
+        base = pl.multiple_of(i * seg, 16)
+        gext[pl.ds(pl.multiple_of(base + top, 8), seg)] = columns(proj, base, seg)
+        rext[pl.ds(pl.multiple_of(base + top, 8), seg)] = proj[pl.ds(base, seg), pl.ds(rec_at, rwid)].astype(f32)
+
+    @pl.when(me.has_down)
+    def _():
+        mail.arrived(halo, rh.at[0], me.partner)
+        gext[pl.ds(0, top)] = columns(halo, 0, top)
+        rext[pl.ds(0, top)] = halo[:, pl.ds(rec_at, rwid)].astype(f32)
+
+    @pl.when(jnp.logical_not(me.has_down))
+    def _():
+        gext[pl.ds(0, top)] = jnp.zeros((top, cw), f32)
+        rext[pl.ds(0, top)] = jnp.zeros((top, rwid), f32)
+
+    softened = rpar[me.q, pl.ds(s_lags + 1, 1), :]
+
+    @pl.loop(0, SEGMENTS)
+    def _(i):
+        base = pl.multiple_of(i * seg, 8)
+        window = rext[pl.ds(pl.multiple_of(base + top - 8, 8), seg + 8)]
+        smooth = jnp.zeros((seg, rwid), f32)
+        for k in range(s_lags + 1):
+            smooth = smooth + rpar[me.q, pl.ds(k, 1), :] * window[8 - s_lags + k : 8 - s_lags + k + seg]
+        smooth = smooth.astype(bf16)
+        gates = jax.nn.sigmoid(jnp.dot(smooth, maps[...], preferred_element_type=f32))
+        retain, admit = gates[:, :rwid], gates[:, fold * 128 : fold * 128 + rwid]
+        log_decay = jump[pl.ds(base, seg)] - retain * softened
+        decay = jnp.exp(log_decay)
+        inflow = jnp.sqrt(minus_expm1(2.0 * log_decay)) * admit * smooth.astype(f32)
+        for f in range(fold):
+            w = min(128, rwid - f * 128)
+            dec[f, pl.ds(base, seg), pl.ds(0, w)] = decay[:, f * 128 : f * 128 + w]
+            inf[f, pl.ds(base, seg), pl.ds(0, w)] = inflow[:, f * 128 : f * 128 + w]
+
+    def one(i, held):
+        after = []
+        for f in range(fold):
+            at = pl.ds(i, SEGMENTS, stride=seg)
+            d = dec.at[f][at, :]
+            product, state = held[2 * f] * d, held[2 * f + 1] * d + inf.at[f][at, :]
+            dec.at[f][at, :] = product
+            inf.at[f][at, :] = state
+            after += [product, state]
+        return tuple(after)
+
+    flat = (SEGMENTS, 128)
+    ends = lax.fori_loop(0, seg, one, (jnp.ones(flat, f32), jnp.zeros(flat, f32)) * fold, unroll=8)
+    for f in range(fold):
+        product, state = jnp.ones((1, 128), f32), jnp.zeros((1, 128), f32)
+        for i in range(SEGMENTS):
+            p, s = ends[2 * f][i : i + 1], ends[2 * f + 1][i : i + 1]
+            product, state = product * p, p * state + s
+        carry[pl.ds(2 * f, 1)] = product
+        carry[pl.ds(2 * f + 1, 1)] = state
+    for device in lined:
+        mail.send(carry, cr_all.at[me.z], rc.at[me.z], device)
+
+    @pl.loop(0, length // 64)
+    def _(i):
+        base = pl.multiple_of(i * 64, 8)
+        window = gext[pl.ds(base, 64 + top)]
+        total = jnp.zeros((64, cw), f32) + cpar[pl.ds(c_lags + 1, 1), :]
+        for k in range(c_lags + 1):
+            begin = top - c_lags + k
+            total = total + cpar[pl.ds(k, 1), :] * window[begin : begin + 64]
+        filt[pl.ds(base, 64)] = total
+        part_sum = jnp.sum(total, axis=1, keepdims=True)
+        off = total - part_sum * (1.0 / cw)
+        lane = lax.broadcasted_iota(jnp.int32, (64, 128), 1)
+        spread = jnp.sum(off * off, axis=1, keepdims=True)
+        stat[pl.ds(base, 64)] = jnp.where(lane == 0, part_sum, spread)
+
+    packed = stat[...].T
+    st_all[mine] = packed[0:8]
+    for device in mates:
+        mail.send(st_all.at[mine], st_all.at[mine], rs.at[mine], device)
 
     def line_step(k):
         for origin, there, on, more in (
@@ -415,34 +490,120 @@
                 mail.send(wz.at[origin], wz.at[origin], rz.at[origin], on, jnp.logical_and(there, more))
             hand_over(wz.at[origin], origin, there)
 
+    for k in range(1, planes):
+        z = (me.z + k) % planes
+        mail.arrived(cr_all.at[z], rc.at[z], me.partner)
+    cr_all[me.z] = carry[...]
+    entering = []
+    for f in range(fold):
+        held = jnp.zeros((1, 128), f32)
+        for j in range(planes - 1):
+            after = cr_all[j, pl.ds(2 * f, 1)] * held + cr_all[j, pl.ds(2 * f + 1, 1)]
+            held = jnp.where(j < me.z, after, held)
+        for i in range(SEGMENTS):
+            entering.append(held)
+            held = ends[2 * f][i : i + 1] * held + ends[2 * f + 1][i : i + 1]
+    own_at = pl.multiple_of(mine * width, 128)
+    for i in range(SEGMENTS):
+        rows = pl.ds(i * seg, seg)
+        state = [dec[f, rows] * entering[f * SEGMENTS + i] + inf[f, rows] for f in range(fold)]
+        state = jnp.concatenate(state, axis=1)[:, :rwid]
+        result = gelu(proj[rows, pl.ds(gate_at, rwid)].astype(f32)) * state
+        fill = jnp.zeros((seg, width - cw - rwid), f32)
+        yall[rows, pl.ds(pl.multiple_of(own_at + cw, 128), width - cw)] = jnp.concatenate([result, fill], axis=1).astype(bf16)
+
+    for k in range(1, 8):
+        d = (mine + k) % 8
+        mail.arrived(st_all.at[d], rs.at[d], me.partner)
+    total = sum(st_all[d, 0:1, :] for d in range(8))
+    mean = total * (1.0 / (8 * cw))
+    spread = jnp.zeros_like(mean)
+    for d in range(8):
+        shift = st_all[d, 0:1, :] * (1.0 / cw) - mean
+        spread = spread + st_all[d, 1:2, :] + cw * shift * shift
+    scale = lax.rsqrt(spread * (1.0 / (8 * cw)) + 1e-05)
+    row = lax.broadcasted_iota(jnp.int32, (128, length), 0)
+    stat[...] = jnp.where(row == 0, mean, scale).T
+
+    @pl.loop(0, SEGMENTS)
+    def _(i):
+        rows = pl.ds(pl.multiple_of(i * seg, 16), seg)
+        pair = stat[rows]
+        v = (filt[rows] - pair[:, 0:1]) * pair[:, 1:2] * cpar[pl.ds(c_lags + 2, 1), :]
+        yall[rows, pl.ds(own_at, cw)] = (v * jax.nn.sigmoid(v)).astype(bf16)
+
+    half_rows = length // 2
+
+    def slot(q, c, h):
+        return yall.at[pl.ds(h * half_rows, half_rows), pl.ds(pl.multiple_of((q * 2 + c) * width, 128), width)]
+
+    yg = PlaneGather(me, mail, lambda h: slot(me.q, me.c, h), slot, ry, rp)
+    yg.start()
+    line_step(1)
     yg.first()
-    line_step(1)
-    yg.second()
     for k in range(2, planes):
-        if k == planes - 1:
-            yg.third()
         line_step(k)
+        if k == 2:
+            yg.second()
+    yg.third()
     yg.last()
     for k in range(part):
         mail.arrived(wp.at[k], rw.at[k], me.partner)
     mail.finish()
 
-
-def middle(planes, mine, weights):
-    rows, width = mine.shape
-    dma = pltpu.SemaphoreType.DMA
+    used, cols = cw + rwid, w_ref.shape[1]
+    tile = length // 8
+
+    @pl.loop(0, 8)
+    def _(i):
+        rows = pl.ds(pl.multiple_of(i * tile, 16), tile)
+        for k in range(part):
+            total = jnp.zeros((tile, cols), f32)
+            for q in range(4):
+                for c, block in ((me.c, wz.at[me.c * part + k]), (1 - me.c, wp.at[k])):
+                    left = yall[rows, pl.ds(pl.multiple_of((q * 2 + c) * width, 128), width)]
+                    total = total + jnp.dot(
+                        left[:, :used], block[pl.ds(q * used, used)], preferred_element_type=f32
+                    )
+            out[i, :, pl.ds(k * cols, cols)] = total.astype(bf16)
+
+
+def core(planes, proj, jump, cpar, rpar, dmap, imap, weights, lags, cw):
+    length, rwid = jump.shape
+    used, cols = cw + rwid, weights.shape[1]
+    width = used + -used % 128
+    fold = (rwid + 127) // 128
+    f32, bf16 = jnp.float32, jnp.bfloat16
+    dma, vmem = pltpu.SemaphoreType.DMA, pltpu.VMEM
+    top = lags[0] + -lags[0] % 16
+    part = planes // 2
     return pl.pallas_call(
-        functools.partial(middle_kernel, planes),
-        out_shape=(
-            jax.ShapeDtypeStruct((rows, 8 * width), mine.dtype),
-            jax.ShapeDtypeStruct((planes,) + weights.shape, weights.dtype),
-            jax.ShapeDtypeStruct((planes // 2,) + weights.shape, weights.dtype),
+        functools.partial(core_kernel, planes, lags),
+        out_shape=jax.ShapeDtypeStruct((8, length // 8, part * cols), bf16),
+        in_specs=[VMEM] * 7,
+        out_specs=VMEM,
+        scratch_shapes=[
+            vmem((planes,) + weights.shape, bf16),
+            vmem((part,) + weights.shape, bf16),
+            vmem((length, 8 * width), bf16),
+            vmem((top, proj.shape[1]), bf16),
+            vmem((top + length, cw), f32),
+            vmem((top + length, rwid), f32),
+            vmem((length, cw), f32),
+            vmem((fold, length, 128), f32),
+            vmem((fold, length, 128), f32),
+            vmem((rwid, 2 * fold * 128), bf16),
+            vmem((length, 128), f32),
+            vmem((8, 8, length), f32),
+            vmem((8, 128), f32),
+            vmem((planes, 8, 128), f32),
+            dma((48 + 8 * planes,)), dma((4, 2)), dma((4, 2)), dma((planes,)), dma((part,)),
+            dma((1,)), dma((8,)), dma((planes,)),
+        ],
+        compiler_params=pltpu.CompilerParams(
+            collective_id=2, has_side_effects=True, vmem_limit_bytes=60 * 1024 * 1024
         ),
-        in_specs=[VMEM] * 2,
-        out_specs=(ANY,) * 3,
-        scratch_shapes=[dma((24 + 5 * planes,)), dma((4, 2)), dma((4, 2)), dma((planes,)), dma((planes // 2,))],
-        compiler_params=pltpu.CompilerParams(collective_id=2, has_side_effects=True),
-    )(mine, weights)
+    )(proj, jump, cpar, rpar, dmap, imap, weights)
 
 
 def leave_kernel(planes, c_ref, out, send, recv):
@@ -471,21 +632,6 @@
         scratch_shapes=[dma((8,)), dma((8,))],
         compiler_params=pltpu.CompilerParams(collective_id=3, has_side_effects=True),
     )(blocks)
-
-
-def scan_kernel(d_ref, u_ref, p_ref, s_ref):
-    def one(i, held):
-        product, state = held
-        decay = d_ref[i]
-        product, state = product * decay, state * decay + u_ref[i]
-        p_ref[i] = product
-        s_ref[i] = state
-        return product, state
-
-    shape = d_ref.shape[1:]
-    lax.fori_loop(
-        0, d_ref.shape[0], one, (jnp.ones(shape, jnp.float32), jnp.zeros(shape, jnp.float32)), unroll=8
-    )
 
 
 def plane_shards(
@@ -527,85 +673,16 @@
     wall = wall.reshape(-1, wall.shape[2])
     jump = jall.reshape(length, rw)
     projected = jnp.dot(xall, wall, preferred_element_type=f32).astype(bf16)
-    glu = glu_of(projected[:, :cw], projected[:, cw : 2 * cw])
-    rec_gate, rec_in = projected[:, 2 * cw : 2 * cw + rw], projected[:, 2 * cw + rw :]
-    conv_lags, short_lags = conv_taps.shape[0] - 1, short_taps.shape[0] - 1
-    edge = passed_along(jnp.concatenate([glu[-conv_lags:], rec_in[-conv_lags:]], axis=1), "sp", 4)
-
-    filtered = causal_window(edge[:, :cw], glu, mine(conv_taps, 1)) + mine(conv_bias, 0)[None, :]
-    local_sum = jnp.sum(filtered, axis=1)
-    off = filtered - (local_sum / cw)[:, None]
-    local_spread = jnp.sum(off * off, axis=1)
-    stats = jnp.stack([local_sum, local_spread]).reshape(-1, 128)
-
-    smoothed = causal_window(edge[-short_lags:, cw:], rec_in, mine(short_taps, 1)).astype(bf16)
-    heads, size = decay_map.shape[0] // 4, decay_map.shape[1]
-    eye = jnp.eye(heads, dtype=bf16)
-
-    def widened(m):
-        return (mine(m, 0)[:, :, None, :] * eye[:, None, :, None]).reshape(rw, rw)
-
-    gates = jax.nn.sigmoid(
-        jnp.dot(
-            smoothed,
-            jnp.concatenate([widened(decay_map), widened(input_map)], axis=1),
-            preferred_element_type=f32,
-        )
-    )
-    retain, admit = gates[:, :rw], gates[:, rw:]
-    log_decay = -RATE_SCALE * retain * jax.nn.softplus(-mine(decay_base, 0))[None, :] + jump
-    decay = jnp.exp(log_decay)
-    inflow = jnp.sqrt(-jnp.expm1(2.0 * log_decay)) * admit * smoothed.astype(f32)
-    steps = length // SEGMENTS
-
-    def by_step(a):
-        return a.reshape(SEGMENTS, steps, rw).transpose(1, 0, 2)
-
-    products, states = pl.pallas_call(
-        scan_kernel,
-        out_shape=(jax.ShapeDtypeStruct((steps, SEGMENTS, rw), f32),) * 2,
-        in_specs=[VMEM] * 2,
-        out_specs=(VMEM,) * 2,
-    )(by_step(decay), by_step(inflow))
-    seg_p, seg_s = products[-1], states[-1]
-    total = (jnp.ones((rw,), f32), jnp.zeros((rw,), f32))
-    for i in range(SEGMENTS):
-        total = chain_step(total, (seg_p[i], seg_s[i]))
-    st_all, cr_all = small(planes, stats, jnp.stack(total))
-
-    st_all = st_all.reshape(8, 2, length)
-    width = 8 * cw
-    mean = jnp.sum(st_all[:, 0], axis=0) / width
-    shift = st_all[:, 0] / cw - mean[None]
-    spread = jnp.sum(st_all[:, 1] + cw * shift * shift, axis=0) / width
-    conv_out = jax.nn.silu(
-        (filtered - mean[:, None]) * lax.rsqrt(spread + 1e-05)[:, None] * mine(conv_gain, 0)[None, :]
-    ).astype(bf16)
-
-    held = jnp.zeros((rw,), f32)
-    for i in range(planes - 1):
-        held = jnp.where(i < z, cr_all[i, 0] * held + cr_all[i, 1], held)
-    entering = []
-    for i in range(SEGMENTS):
-        entering.append(held)
-        held = seg_p[i] * held + seg_s[i]
-    state = (states + products * jnp.stack(entering)[None]).transpose(1, 0, 2).reshape(length, rw)
-    rec_out = (jax.nn.gelu(rec_gate.astype(f32)) * state).astype(bf16)
-    fill = -(cw + rw) % 128
-    block = jnp.concatenate([conv_out, rec_out, jnp.zeros((length, fill), bf16)], axis=1)
-
     cols = out_conv_w.shape[1]
     rows_by_mate = jnp.concatenate(
         [out_conv_w.reshape(4, cw, cols), out_rec_w.reshape(4, rw, cols)], axis=1
     ).reshape(-1, cols)
-    yall, wz, wp = middle(planes, block, rows_by_mate)
+    cpar = mine(jnp.concatenate([conv_taps.astype(f32), conv_bias[None], conv_gain[None]]), 1)
+    rpar = by_mate(jnp.concatenate([short_taps.astype(f32), RATE_SCALE * jax.nn.softplus(-decay_base)[None]]))
+    lags = (conv_taps.shape[0] - 1, short_taps.shape[0] - 1)
+    mixed = core(planes, projected, jump, cpar, rpar, decay_map, input_map, rows_by_mate, lags, cw)
+    out = leave(planes, mixed)
     part = planes // 2
-    own = lax.dynamic_slice_in_dim(wz, c * part, part, 0)
-    both = jnp.stack([jnp.where(c == 0, own, wp), jnp.where(c == 0, wp, own)])
-    both = both.reshape(2, part, 4, cw + rw, cols).transpose(2, 0, 3, 1, 4)
-    both = jnp.pad(both, ((0, 0), (0, 0), (0, fill), (0, 0), (0, 0))).reshape(-1, part * cols)
-    mixed = jnp.dot(yall, both, preferred_element_type=f32).astype(bf16)
-    out = leave(planes, mixed.reshape(8, length // 8, part * cols))
     out = out.reshape(4, 2, length // 8, part, cols).transpose(2, 1, 3, 0, 4)
     return out.reshape(length // 8, -1)
 

time: 268 us -> 233 us (0.87)
  other arithmetic: 31.1 us -> 7.98 us
  local copies, waits for them, and re-layouts: 32.9 us -> 10.5 us
  Pallas kernels: 178 us -> 198 us
  matrix products: 21.9 us -> 15.4 us
  starting transfers between devices: 2.85 us -> 0 us
    pallas_call x3 -> x1, Pallas kernels: 61.4 us -> 82 us  [core(): pl.pallas_call(functools.partial(core_kernel, planes, lags), out_shape=ja...]
    dot_general x2 -> x0, matrix products: 7.52 us -> none  [the longest x1 6.36 us: plane_shards(): mixed = jnp.dot(yall, both, preferred_element_type=f32).astype(bf16)]
    reshape x4 -> x0, local copies, waits for them, and re-layouts: 5.69 us -> none  [the longest x2 4.13 us: by_step(): return a.reshape(SEGMENTS, steps, rw).transpose(1, 0, 2)]
    transpose x2 -> x1, other arithmetic: 5.83 us -> 0.61 us  [by_mate(): return a.reshape(a.shape[0], 4, a.shape[1] // 4).transpose(1, 0, 2)]
    reduce_sum x4 -> x0, other arithmetic: 4.74 us -> none  [the longest x1 4.12 us: plane_shards(): local_sum = jnp.sum(filtered, axis=1)]
    mul x4 -> x1, other arithmetic: 3.94 us -> 0.01 us  [plane_shards(): RATE_SCALE * jax.nn.softplus(-decay_base)[None]]
    dynamic_slice x3 -> x0, local copies, waits for them, and re-layouts: 3.47 us -> none  [mine(): return lax.dynamic_slice_in_dim(a, q * size, size, axis)]
    convert_element_type x8 -> x1, other arithmetic: 3.04 us -> 0.01 us  [plane_shards(): conv_taps.astype(f32)]
  transfers between devices with their start and end apart: 1 -> 0, of which waited for: 0 -> 0; matrix products, arithmetic and copies ran while one was open for 4% -> 0% of each run, Pallas kernels for 0% -> 0%
where the time goes in v2:
time: 233 us
  Pallas kernels  198 us (85%)
  matrix products  15.4 us (7%)
  local copies, waits for them, and re-layouts  10.5 us (5%)
  other arithmetic  7.98 us (3%)
    pallas_call x1, Pallas kernels, enter(): pl.pallas_call(functools.partial(enter_kernel, planes), out_shape=(jax.Sh...  94.4 us
    pallas_call x1, Pallas kernels, core(): pl.pallas_call(functools.partial(core_kernel, planes, lags), out_shape=ja...  82 us
    pallas_call x1, Pallas kernels, leave(): pl.pallas_call(functools.partial(leave_kernel, planes), out_shape=jax.Sha...  22 us
    dot_general x1, matrix products, plane_shards(): projected = jnp.dot(xall, wall, preferred_element_type=f32).astype(bf16)  15.4 us

profile of v2, /device:TPU:0, one launch (start us, length us, event | category | flops | bytes accessed | tf_op | source)
XLA Modules:
  0.0 232.6 jit_solution(17337396756456267378)
XLA Ops:
  0.0 1.9 fusion
  1.9 0.0 copy-start.3
  2.0 2.4 %fusion.2.x_ref = bf16[192,4096]{1,0:T(8,128)(2,1)} fusion(bf16[192,4096]{1,0:T(8,128)(2,1)S(1)} %copy-done, f32[4096]{0:T(1024)} %param.17, f32[192]{0:T(256)S(1)} %add_rsqrt_fusion), kind=kLoop, calls=%fused_computation.5 | loop fusion | flops 3145728 | bytes 3162880 | tf_op jit(solution)/shard_map/convert_element_type | solution.py:38
  4.4 0.2 copy.24
  4.5 0.0 copy-start.7
  4.6 0.2 copy.25
  4.8 0.2 copy.22
  4.9 0.2 copy.23
  5.2 0.2 copy-done.6
  5.3 0.1 copy.20
  5.5 0.2 copy.21
  5.7 0.1 copy.18
  5.8 0.2 copy.19
  6.0 1.5 pad_maximum_fusion.w_ref
  7.4 0.4 copy.26
  7.8 1.7 copy.27
  9.5 94.4 %shard_map.154 = (bf16[8,192,4096]{2,1,0:T(8,128)(2,1)}, bf16[16,256,640]{2,1,0:T(8,128)(2,1)}, f32[4,384,192]{2,1,0:T(8,128)}) custom-call(bf16[192,4096]{1,0:T(8,128)(2,1)} %fusion.2.x_ref, bf16[4,256,640]{2,1,0:T(8,128)(2,1)} %pad_maximum_fusion.w_ref, f32[4,384,192]{2,1,0:T(8,128)} %bitcast.24), custom_call_target="tpu_custom_call" | custom-call | tf_op jit(solution)/shard_map/pallas_call | solution.py:328
  103.9 0.0 copy-start.12
  103.9 0.0 copy-start.10
  103.9 0.0 copy-start.4
  103.9 0.0 copy-start.5
  104.0 15.4 %convolution_convert_fusion.proj = bf16[1536,640]{1,0:T(8,128)(2,1)} fusion(bf16[1536,4096]{1,0:T(8,128)(2,1)} %bitcast.40, bf16[4096,640]{1,0:T(8,128)(2,1)} %bitcast.41), kind=kOutput, calls=%fused_computation.2 | convolution fusion | flops 8054046720 | bytes 19791872 | tf_op jit(solution)/shard_map/dot_general | solution.py:675
  119.4 0.7 fusion.4.cpar
  120.1 0.1 concatenate.23
  120.2 0.1 reshape.67
  120.3 0.6 maximum_bitcast_fusion.rpar
  120.9 0.9 pad_maximum_fusion.1
  121.8 82.0 %shard_map.155.c_ref = bf16[8,192,512]{2,1,0:T(8,128)(2,1)} custom-call(bf16[1536,640]{1,0:T(8,128)(2,1)} %convolution_convert_fusion.proj, f32[1536,192]{1,0:T(8,128)} %bitcast.31, f32[33,128]{1,0:T(8,128)} %fusion.4.cpar, f32[4,5,192]{2,1,0:T(8,128)} %maximum_bitcast_fusion.rpar, bf16[12,64,64]{2,1,0:T(8,128)(2,1)} %dmap.1, bf16[12,64,64]{2,1,0:T(8,128)(2,1)} %imap.1, ...), custom_call_target="tpu_custom_call" | custom-call | tf_op jit(solution)/shard_map/pallas_call | solution.py:580
  203.8 22.0 %shard_map.156 = bf16[8,192,512]{2,1,0:T(8,128)(2,1)} custom-call(bf16[8,192,512]{2,1,0:T(8,128)(2,1)} %shard_map.155.c_ref), custom_call_target="tpu_custom_call" | custom-call | tf_op jit(solution)/shard_map/pallas_call | solution.py:627
  225.8 2.4 %reshape.65 = bf16[4,2,192,2,256]{4,3,2,1,0:T(2,128)(2,1)S(1)} reshape(bf16[8,192,512]{2,1,0:T(8,128)(2,1)} %shard_map.156) | data formatting | bytes 3145728 | tf_op jit(solution)/shard_map/reshape | solution.py:686
  228.2 2.0 copy.29
  230.2 2.4 %reshape.66 = bf16[192,4096]{1,0:T(8,128)(2,1)} reshape(bf16[192,2,2,4,256]{4,3,2,1,0:T(4,128)(2,1)S(1)} %copy.29) | data formatting | bytes 3145728 | tf_op jit(solution)/shard_map/reshape | solution.py:687
  (23 shorter events, 0.1 us)
Async XLA Ops:
  0.0 1.9 copy-start
  1.9 2.4 %copy-start.2 = (bf16[256,768]{1,0:T(8,128)(2,1)S(1)}, bf16[256,768]{1,0:T(8,128)(2,1)}, u32[]{:S(2)}) copy-start(bf16[256,768]{1,0:T(8,128)(2,1)} %param.21) | copy-start | bytes 1179652
  1.9 2.8 %copy-start.3 = (bf16[256,768]{1,0:T(8,128)(2,1)S(1)}, bf16[256,768]{1,0:T(8,128)(2,1)}, u32[]{:S(2)}) copy-start(bf16[256,768]{1,0:T(8,128)(2,1)} %param.20) | copy-start | bytes 1179652
  4.4 1.0 copy-start.6
  4.5 1.1 copy-start.7
  5.6 1.8 copy-start.1
  103.9 15.5 %copy-start.8 = (bf16[31,512]{1,0:T(8,128)(2,1)S(1)}, bf16[31,512]{1,0:T(8,128)(2,1)}, u32[]{:S(2)}) copy-start(bf16[31,512]{1,0:T(8,128)(2,1)} %param.22) | copy-start | bytes 95236
  103.9 15.5 %copy-start.11 = (f32[512]{0:T(512)S(1)}, f32[512]{0:T(512)}, u32[]{:S(2)}) copy-start(f32[512]{0:T(512)} %param.23) | copy-start | bytes 6148
  103.9 15.5 %copy-start.12 = (f32[512]{0:T(512)S(1)}, f32[512]{0:T(512)}, u32[]{:S(2)}) copy-start(f32[512]{0:T(512)} %param.24) | copy-start | bytes 6148
  103.9 16.2 %copy-start.10 = (f32[768]{0:T(1024)S(1)}, f32[768]{0:T(1024)}, u32[]{:S(2)}) copy-start(f32[768]{0:T(1024)} %param.28) | copy-start | bytes 9220
  103.9 16.3 %copy-start.9 = (bf16[4,768]{1,0:T(4,128)(2,1)S(1)}, bf16[4,768]{1,0:T(4,128)(2,1)}, u32[]{:S(2)}) copy-start(bf16[4,768]{1,0:T(4,128)(2,1)} %param.25) | copy-start | bytes 18436
  103.9 17.0 %copy-start.4 = (bf16[768,256]{1,0:T(8,128)(2,1)S(1)}, bf16[768,256]{1,0:T(8,128)(2,1)}, u32[]{:S(2)}) copy-start(bf16[768,256]{1,0:T(8,128)(2,1)} %param.31) | copy-start | bytes 1179652
  103.9 17.0 %copy-start.5 = (bf16[512,256]{1,0:T(8,128)(2,1)S(1)}, bf16[512,256]{1,0:T(8,128)(2,1)}, u32[]{:S(2)}) copy-start(bf16[512,256]{1,0:T(8,128)(2,1)} %param.30) | copy-start | bytes 786436

commit v3 on v2

--- a/solution.py
+++ b/solution.py
@@ -265,35 +265,49 @@
                 self.mail.arrived(self.slot(q, 1 - me.c, half), self.recv_pair.at[q, half], me.partner)
 
 
-def enter_kernel(planes, x_ref, w_ref, j_ref, xall, wall, jall, send, rx, rp, rw, rz, rj):
+def enter_kernel(
+    planes, x_ref, gain, w_ref, j_ref, proj, jall, xall, wall, acc, send, rx, rp, rw, rz, rj
+):
     me = Spot(planes)
     mail = Mail(send)
     greet(me, [me.mate(me.qx), me.mate(me.qy), me.mate(me.qd), me.partner], True)
     others = (me.qx, me.qy, me.qd)
+    depth = w_ref.shape[1]
+    rows = x_ref.shape[0]
+
+    def wslot(origin, piece):
+        return wall.at[pl.ds(pl.multiple_of((origin * 4 + piece) * depth, depth), depth)]
 
     def to_line(src, origin, piece):
-        index = origin * 4 + piece
-        mail.send(src, wall.at[index], rz.at[origin, piece], me.up, me.has_up)
-        mail.send(src, wall.at[index], rz.at[origin, piece], me.down, me.has_down)
+        mail.send(src, wslot(origin, piece), rz.at[origin, piece], me.up, me.has_up)
+        mail.send(src, wslot(origin, piece), rz.at[origin, piece], me.down, me.has_down)
 
     for q in others:
-        mail.send(w_ref.at[q], wall.at[me.s], rw.at[me.q], me.mate(q))
+        mail.send(w_ref.at[q], wslot(me.z, me.q), rw.at[me.q], me.mate(q))
     to_line(w_ref.at[me.q], me.z, me.q)
-    half_rows = x_ref.shape[0] // 2
-    xg = PlaneGather(
-        me, mail,
-        lambda h: x_ref.at[pl.ds(h * half_rows, half_rows)],
-        lambda q, c, h: xall.at[q * 2 + c, pl.ds(h * half_rows, half_rows)],
-        rx, rp,
-    )
+    mail.local(w_ref.at[me.q], wslot(me.z, me.q))
+
+    first_row = (me.q * 2 + me.c) * rows
+
+    @pl.loop(0, rows // 16)
+    def _(i):
+        values = x_ref[pl.ds(pl.multiple_of(i * 16, 16), 16)].astype(jnp.float32)
+        inverse = lax.rsqrt(jnp.mean(values * values, axis=1, keepdims=True) + 1e-06)
+        place = pl.ds(pl.multiple_of(first_row + i * 16, 16), 16)
+        xall[place] = (values * inverse * gain[...]).astype(xall.dtype)
+
+    half_rows = rows // 2
+
+    def slot(q, c, h):
+        return xall.at[pl.ds(pl.multiple_of((q * 2 + c) * rows + h * half_rows, 16), half_rows)]
+
+    xg = PlaneGather(me, mail, lambda h: slot(me.q, me.c, h), slot, rx, rp)
     xg.start()
     for q in others:
         mail.send(j_ref.at[q], jall.at[me.q], rj.at[me.q], me.mate(q))
-    mail.local(x_ref, xall.at[me.q * 2 + me.c])
-    mail.local(w_ref.at[me.q], wall.at[me.s])
     mail.local(j_ref.at[me.q], jall.at[me.q])
     for q in others:
-        here = wall.at[me.z * 4 + q]
+        here = wslot(me.z, q)
         mail.arrived(here, rw.at[q], me.partner)
         to_line(here, me.z, q)
 
@@ -303,11 +317,10 @@
                 (me.z - k, me.z >= k, me.up, me.has_up),
                 (me.z + k, me.z + k < planes, me.down, me.has_down),
             ):
-                here = wall.at[origin * 4 + piece]
+                here = wslot(origin, piece)
                 sem = rz.at[origin, piece]
                 pl.when(there)(functools.partial(mail.arrived, here, sem, me.partner))
-                if k < planes - 1:
-                    mail.send(here, here, sem, on, jnp.logical_and(there, more))
+                mail.send(here, here, sem, on, jnp.logical_and(there, more))
 
     line_step(1)
     xg.first()
@@ -317,26 +330,59 @@
     for q in others:
         mail.arrived(jall.at[q], rj.at[q], me.partner)
     xg.third()
-    line_step(planes - 1)
     xg.last()
     mail.finish()
-
-
-def enter(planes, normed, pieces, jumps):
-    rows, width = normed.shape
-    dma = pltpu.SemaphoreType.DMA
+    tile = acc.shape[0] // 4
+
+    def multiply(start, size, fresh=False):
+        at = pl.ds(pl.multiple_of(start, depth), size)
+
+        @pl.loop(0, 4)
+        def _(i):
+            part = pl.ds(pl.multiple_of(i * tile, 16), tile)
+            product = jnp.dot(xall[part, at], wall[at], preferred_element_type=jnp.float32)
+            acc[part] = product if fresh else acc[part] + product
+
+    multiply(me.z * 4 * depth, 4 * depth, True)
+    for k in range(1, planes - 1):
+        for origin, there in ((me.z - k, me.z >= k), (me.z + k, me.z + k < planes)):
+            pl.when(there)(functools.partial(multiply, origin * 4 * depth, 4 * depth))
+    far = planes - 1 - me.z
+
+    @pl.when(jnp.logical_or(me.z == 0, me.z == planes - 1))
+    def _():
+        for piece in (me.q,) + others:
+            mail.arrived(wslot(far, piece), rz.at[far, piece], me.partner)
+            multiply((far * 4 + piece) * depth, depth)
+
+    @pl.loop(0, 8)
+    def _(i):
+        part = pl.ds(pl.multiple_of(i * (tile // 2), 16), tile // 2)
+        proj[part] = acc[part].astype(proj.dtype)
+
+
+def enter(planes, tokens, gain, pieces, jumps):
+    rows, width = tokens.shape
+    depth, cols = pieces.shape[1:]
+    dma, vmem = pltpu.SemaphoreType.DMA, pltpu.VMEM
     return pl.pallas_call(
         functools.partial(enter_kernel, planes),
         out_shape=(
-            jax.ShapeDtypeStruct((8, rows, width), normed.dtype),
-            jax.ShapeDtypeStruct((planes * 4,) + pieces.shape[1:], pieces.dtype),
+            jax.ShapeDtypeStruct((8 * rows, cols), tokens.dtype),
             jax.ShapeDtypeStruct(jumps.shape, jumps.dtype),
         ),
-        in_specs=[VMEM] * 3,
-        out_specs=(ANY,) * 3,
-        scratch_shapes=[dma((40 + 8 * planes,)), dma((4, 2)), dma((4, 2)), dma((4,)), dma((planes, 4)), dma((4,))],
-        compiler_params=pltpu.CompilerParams(collective_id=0, has_side_effects=True),
-    )(normed, pieces, jumps)
+        in_specs=[VMEM] * 4,
+        out_specs=(VMEM,) * 2,
+        scratch_shapes=[
+            vmem((8 * rows, width), tokens.dtype),
+            vmem((planes * 4 * depth, cols), pieces.dtype),
+            vmem((8 * rows, cols), jnp.float32),
+            dma((40 + 8 * planes,)), dma((4, 2)), dma((4, 2)), dma((4,)), dma((planes, 4)), dma((4,)),
+        ],
+        compiler_params=pltpu.CompilerParams(
+            collective_id=0, has_side_effects=True, vmem_limit_bytes=56 * 1024 * 1024
+        ),
+    )(tokens, gain, pieces, jumps)
 
 
 def minus_expm1(y):
@@ -352,8 +398,8 @@
 
 def core_kernel(
     planes, lags, proj, jump, cpar, rpar, dmap, imap, w_ref,
-    out, wz, wp, yall, halo, gext, rext, filt, dec, inf, maps, stat, st_all, carry, cr_all,
-    send, ry, rp, rz, rw, rh, rs, rc,
+    out, wz, wp, yall, cbuf, halo, gext, rext, filt, dec, inf, maps, stat, st_all, carry, cr_all,
+    send, ry, rp, rv, rq, rz, rw, rh, rs, rc, ls, lr,
 ):
     me = Spot(planes)
     mail = Mail(send)
@@ -403,18 +449,15 @@
     @pl.loop(0, SEGMENTS)
     def _(i):
         base = pl.multiple_of(i * seg, 16)
-        gext[pl.ds(pl.multiple_of(base + top, 8), seg)] = columns(proj, base, seg)
         rext[pl.ds(pl.multiple_of(base + top, 8), seg)] = proj[pl.ds(base, seg), pl.ds(rec_at, rwid)].astype(f32)
 
     @pl.when(me.has_down)
     def _():
         mail.arrived(halo, rh.at[0], me.partner)
-        gext[pl.ds(0, top)] = columns(halo, 0, top)
         rext[pl.ds(0, top)] = halo[:, pl.ds(rec_at, rwid)].astype(f32)
 
     @pl.when(jnp.logical_not(me.has_down))
     def _():
-        gext[pl.ds(0, top)] = jnp.zeros((top, cw), f32)
         rext[pl.ds(0, top)] = jnp.zeros((top, rwid), f32)
 
     softened = rpar[me.q, pl.ds(s_lags + 1, 1), :]
@@ -460,25 +503,18 @@
     for device in lined:
         mail.send(carry, cr_all.at[me.z], rc.at[me.z], device)
 
-    @pl.loop(0, length // 64)
-    def _(i):
-        base = pl.multiple_of(i * 64, 8)
-        window = gext[pl.ds(base, 64 + top)]
-        total = jnp.zeros((64, cw), f32) + cpar[pl.ds(c_lags + 1, 1), :]
-        for k in range(c_lags + 1):
-            begin = top - c_lags + k
-            total = total + cpar[pl.ds(k, 1), :] * window[begin : begin + 64]
-        filt[pl.ds(base, 64)] = total
-        part_sum = jnp.sum(total, axis=1, keepdims=True)
-        off = total - part_sum * (1.0 / cw)
-        lane = lax.broadcasted_iota(jnp.int32, (64, 128), 1)
-        spread = jnp.sum(off * off, axis=1, keepdims=True)
-        stat[pl.ds(base, 64)] = jnp.where(lane == 0, part_sum, spread)
-
-    packed = stat[...].T
-    st_all[mine] = packed[0:8]
-    for device in mates:
-        mail.send(st_all.at[mine], st_all.at[mine], rs.at[mine], device)
+    @pl.loop(0, SEGMENTS)
+    def _(i):
+        base = pl.multiple_of(i * seg, 16)
+        gext[pl.ds(pl.multiple_of(base + top, 8), seg)] = columns(proj, base, seg)
+
+    @pl.when(me.has_down)
+    def _():
+        gext[pl.ds(0, top)] = columns(halo, 0, top)
+
+    @pl.when(jnp.logical_not(me.has_down))
+    def _():
+        gext[pl.ds(0, top)] = jnp.zeros((top, cw), f32)
 
     def line_step(k):
         for origin, there, on, more in (
@@ -512,6 +548,39 @@
         fill = jnp.zeros((seg, width - cw - rwid), f32)
         yall[rows, pl.ds(pl.multiple_of(own_at + cw, 128), width - cw)] = jnp.concatenate([result, fill], axis=1).astype(bf16)
 
+    half_rows = length // 2
+
+    def gather(lane, lanes, recv, recv_pair):
+        def slot(q, c, h):
+            spot = pl.ds(pl.multiple_of((q * 2 + c) * width + lane, 128), lanes)
+            return yall.at[pl.ds(h * half_rows, half_rows), spot]
+
+        return PlaneGather(me, mail, lambda h: slot(me.q, me.c, h), slot, recv, recv_pair)
+
+    vg = gather(cw, width - cw, rv, rq)
+    vg.start()
+
+    @pl.loop(0, length // 64)
+    def _(i):
+        base = pl.multiple_of(i * 64, 8)
+        window = gext[pl.ds(base, 64 + top)]
+        total = jnp.zeros((64, cw), f32) + cpar[pl.ds(c_lags + 1, 1), :]
+        for k in range(c_lags + 1):
+            begin = top - c_lags + k
+            total = total + cpar[pl.ds(k, 1), :] * window[begin : begin + 64]
+        filt[pl.ds(base, 64)] = total
+        part_sum = jnp.sum(total, axis=1, keepdims=True)
+        off = total - part_sum * (1.0 / cw)
+        lane = lax.broadcasted_iota(jnp.int32, (64, 128), 1)
+        spread = jnp.sum(off * off, axis=1, keepdims=True)
+        stat[pl.ds(base, 64)] = jnp.where(lane == 0, part_sum, spread)
+
+    packed = stat[...].T
+    st_all[mine] = packed[0:8]
+    for device in mates:
+        mail.send(st_all.at[mine], st_all.at[mine], rs.at[mine], device)
+
+    line_step(1)
     for k in range(1, 8):
         d = (mine + k) % 8
         mail.arrived(st_all.at[d], rs.at[d], me.partner)
@@ -532,31 +601,28 @@
         v = (filt[rows] - pair[:, 0:1]) * pair[:, 1:2] * cpar[pl.ds(c_lags + 2, 1), :]
         yall[rows, pl.ds(own_at, cw)] = (v * jax.nn.sigmoid(v)).astype(bf16)
 
-    half_rows = length // 2
-
-    def slot(q, c, h):
-        return yall.at[pl.ds(h * half_rows, half_rows), pl.ds(pl.multiple_of((q * 2 + c) * width, 128), width)]
-
-    yg = PlaneGather(me, mail, lambda h: slot(me.q, me.c, h), slot, ry, rp)
+    yg = gather(0, cw, ry, rp)
     yg.start()
-    line_step(1)
+    vg.first()
     yg.first()
-    for k in range(2, planes):
+    for k in range(2, planes - 1):
         line_step(k)
-        if k == 2:
-            yg.second()
+    vg.second()
+    yg.second()
+    vg.third()
     yg.third()
-    yg.last()
+    line_step(planes - 1)
     for k in range(part):
         mail.arrived(wp.at[k], rw.at[k], me.partner)
+    vg.last()
+    yg.last()
     mail.finish()
 
     used, cols = cw + rwid, w_ref.shape[1]
     tile = length // 8
 
-    @pl.loop(0, 8)
-    def _(i):
-        rows = pl.ds(pl.multiple_of(i * tile, 16), tile)
+    def multiply(d):
+        rows = pl.ds(pl.multiple_of(d * tile, 16), tile)
         for k in range(part):
             total = jnp.zeros((tile, cols), f32)
             for q in range(4):
@@ -565,7 +631,44 @@
                     total = total + jnp.dot(
                         left[:, :used], block[pl.ds(q * used, used)], preferred_element_type=f32
                     )
-            out[i, :, pl.ds(k * cols, cols)] = total.astype(bf16)
+            cbuf[d, k] = total.astype(bf16)
+
+    def place(q, c, k):
+        return out.at[:, pl.ds(pl.multiple_of(((c * part + k) * 4 + q) * cols, 128), cols)]
+
+    def target(i):
+        flip = 3 - i // 2
+        q = (me.q // 2 + flip // 2) % 2 * 2 + (me.q % 2 + flip % 2) % 2
+        return q, (me.c + 1 + i) % 2
+
+    def parcel(i, k):
+        q, c = target(i)
+        return pltpu.make_async_remote_copy(
+            src_ref=cbuf.at[q * 2 + c, k], dst_ref=place(me.q, me.c, k), send_sem=ls.at[i, k],
+            recv_sem=lr.at[mine, k], device_id=me.at(me.z * 4 + q, c), device_id_type=MESH,
+        )
+
+    @pl.loop(0, 7)
+    def _(i):
+        q, c = target(i)
+        multiply(q * 2 + c)
+        for k in range(part):
+            parcel(i, k).start()
+
+    multiply(mine)
+    kept = [pltpu.make_async_copy(cbuf.at[mine, k], place(me.q, me.c, k), ls.at[7, k]) for k in range(part)]
+    for copy in kept:
+        copy.start()
+
+    @pl.loop(0, 7)
+    def _(i):
+        q, c = target(i)
+        for k in range(part):
+            mail.arrived(place(q, c, k), lr.at[q * 2 + c, k], me.partner)
+            parcel(i, k).wait_send()
+
+    for copy in kept:
+        copy.wait()
 
 
 def core(planes, proj, jump, cpar, rpar, dmap, imap, weights, lags, cw):
@@ -579,13 +682,14 @@
     part = planes // 2
     return pl.pallas_call(
         functools.partial(core_kernel, planes, lags),
-        out_shape=jax.ShapeDtypeStruct((8, length // 8, part * cols), bf16),
+        out_shape=jax.ShapeDtypeStruct((length // 8, planes * 4 * cols), bf16),
         in_specs=[VMEM] * 7,
-        out_specs=VMEM,
+        out_specs=ANY,
         scratch_shapes=[
             vmem((planes,) + weights.shape, bf16),
             vmem((part,) + weights.shape, bf16),
             vmem((length, 8 * width), bf16),
+            vmem((8, part, length // 8, cols), bf16),
             vmem((top, proj.shape[1]), bf16),
             vmem((top + length, cw), f32),
             vmem((top + length, rwid), f32),
@@ -597,41 +701,13 @@
             vmem((8, 8, length), f32),
             vmem((8, 128), f32),
             vmem((planes, 8, 128), f32),
-            dma((48 + 8 * planes,)), dma((4, 2)), dma((4, 2)), dma((planes,)), dma((part,)),
-            dma((1,)), dma((8,)), dma((planes,)),
+            dma((64 + 8 * planes,)), dma((4, 2)), dma((4, 2)), dma((4, 2)), dma((4, 2)), dma((planes,)), dma((part,)),
+            dma((1,)), dma((8,)), dma((planes,)), dma((8, part)), dma((8, part)),
         ],
         compiler_params=pltpu.CompilerParams(
             collective_id=2, has_side_effects=True, vmem_limit_bytes=60 * 1024 * 1024
         ),
     )(proj, jump, cpar, rpar, dmap, imap, weights)
-
-
-def leave_kernel(planes, c_ref, out, send, recv):
-    me = Spot(planes)
-    mail = Mail(send)
-    mine = me.q * 2 + me.c
-    mates = [((me.q + dq) % 4, c) for dq in (3, 1, 2, 0) for c in (me.c, 1 - me.c)]
-    mates = [(q, c) for i, (q, c) in enumerate(mates) if i != 6]
-    devices = [me.at(me.z * 4 + q, c) for q, c in mates]
-    greet(me, devices, False)
-    for (q, c), device in zip(mates, devices):
-        mail.send(c_ref.at[q * 2 + c], out.at[mine], recv.at[mine], device)
-    mail.local(c_ref.at[mine], out.at[mine])
-    for q, c in mates:
-        mail.arrived(out.at[q * 2 + c], recv.at[q * 2 + c], me.partner)
-    mail.finish()
-
-
-def leave(planes, blocks):
-    dma = pltpu.SemaphoreType.DMA
-    return pl.pallas_call(
-        functools.partial(leave_kernel, planes),
-        out_shape=jax.ShapeDtypeStruct(blocks.shape, blocks.dtype),
-        in_specs=[VMEM],
-        out_specs=ANY,
-        scratch_shapes=[dma((8,)), dma((8,))],
-        compiler_params=pltpu.CompilerParams(collective_id=3, has_side_effects=True),
-    )(blocks)
 
 
 def plane_shards(
@@ -653,9 +729,9 @@
     out_conv_w,
     out_rec_w,
 ):
-    s, c = lax.axis_index("sp"), lax.axis_index("tp")
-    z, q = s // 4, s % 4
-    f32, bf16 = jnp.float32, jnp.bfloat16
+    s = lax.axis_index("sp")
+    q = s % 4
+    f32 = jnp.float32
 
     def by_mate(a):
         return a.reshape(a.shape[0], 4, a.shape[1] // 4).transpose(1, 0, 2)
@@ -664,15 +740,10 @@
         size = a.shape[axis] // 4
         return lax.dynamic_slice_in_dim(a, q * size, size, axis)
 
-    normed = norm_rows(tokens, norm_gain)
     pieces = jnp.concatenate([by_mate(w) for w in (conv_val_w, conv_gate_w, rec_gate_w, rec_in_w)], axis=2)
-    xall, wall, jall = enter(planes, normed, pieces, by_mate(decay_jump))
-    length = xall.shape[0] * xall.shape[1]
+    projected, jall = enter(planes, tokens, norm_gain[None], pieces, by_mate(decay_jump))
     cw, rw = conv_val_w.shape[1] // 4, rec_in_w.shape[1] // 4
-    xall = xall.reshape(length, xall.shape[2])
-    wall = wall.reshape(-1, wall.shape[2])
-    jump = jall.reshape(length, rw)
-    projected = jnp.dot(xall, wall, preferred_element_type=f32).astype(bf16)
+    jump = jall.reshape(-1, rw)
     cols = out_conv_w.shape[1]
     rows_by_mate = jnp.concatenate(
         [out_conv_w.reshape(4, cw, cols), out_rec_w.reshape(4, rw, cols)], axis=1
@@ -680,11 +751,7 @@
     cpar = mine(jnp.concatenate([conv_taps.astype(f32), conv_bias[None], conv_gain[None]]), 1)
     rpar = by_mate(jnp.concatenate([short_taps.astype(f32), RATE_SCALE * jax.nn.softplus(-decay_base)[None]]))
     lags = (conv_taps.shape[0] - 1, short_taps.shape[0] - 1)
-    mixed = core(planes, projected, jump, cpar, rpar, decay_map, input_map, rows_by_mate, lags, cw)
-    out = leave(planes, mixed)
-    part = planes // 2
-    out = out.reshape(4, 2, length // 8, part, cols).transpose(2, 1, 3, 0, 4)
-    return out.reshape(length // 8, -1)
+    return core(planes, projected, jump, cpar, rpar, decay_map, input_map, rows_by_mate, lags, cw)
 
 
 def solution(mesh):
@@ -708,6 +775,6 @@
     )
     out_specs = P(("sp", "tp"), None)
     count = mesh.shape["sp"]
-    planar = mesh.shape["tp"] == 2 and count % 8 == 0
+    planar = mesh.shape["tp"] == 2 and count % 8 == 0 and count >= 16
     body = functools.partial(plane_shards, count // 4) if planar else shards
     return jax.shard_map(body, mesh=mesh, in_specs=in_specs, out_specs=out_specs, check_vma=False)

time: 233 us -> 216 us (0.927)
  matrix products: 15.4 us -> 0 us
  Pallas kernels: 198 us -> 204 us
  other arithmetic: 7.98 us -> 3.59 us
  local copies, waits for them, and re-layouts: 10.5 us -> 7.55 us
    pallas_call x1 -> x0, Pallas kernels: 22 us -> none  [leave(): pl.pallas_call(functools.partial(leave_kernel, planes), out_shape=jax.Sha...]
    dot_general x1 -> x0, matrix products: 15.4 us -> none  [plane_shards(): projected = jnp.dot(xall, wall, preferred_element_type=f32).astype(bf16)]
    pallas_call x1, Pallas kernels: 94.4 us -> 109 us  [enter(): pl.pallas_call(functools.partial(enter_kernel, planes), out_shape=(jax.Sh...]
    pallas_call x1, Pallas kernels: 82 us -> 94.7 us  [core(): pl.pallas_call(functools.partial(core_kernel, planes, lags), out_shape=ja...]
    reshape x2 -> x0, local copies, waits for them, and re-layouts: 4.74 us -> none  [the longest x1 2.38 us: plane_shards(): return out.reshape(length // 8, -1)]
    unnamed x31 -> x28, local copies, waits for them, and re-layouts: 1.2 us -> 5 us
    convert_element_type x1 -> x0, other arithmetic: 2.4 us -> none  [norm_rows(): return (widened * inverse * gain).astype(jnp.bfloat16)]
where the time goes in v3:
time: 216 us; the launch traced here: 215 us
  Pallas kernels  204 us (94%)
  local copies, waits for them, and re-layouts  7.55 us (3%)
  other arithmetic  3.59 us (2%)
    pallas_call x1, Pallas kernels, enter(): pl.pallas_call(functools.partial(enter_kernel, planes), out_shape=(jax.Sh...  109 us
    pallas_call x1, Pallas kernels, core(): pl.pallas_call(functools.partial(core_kernel, planes, lags), out_shape=ja...  94.7 us
    unnamed x28, local copies, waits for them, and re-layouts  5 us

profile of v3, /device:TPU:0, one launch (start us, length us, event | category | flops | bytes accessed | tf_op | source)
XLA Modules:
  0.0 215.3 jit_solution(3883130075807793209)
XLA Ops:
  0.0 1.2 copy.23
  1.2 0.2 copy.24
  1.4 0.0 copy-start.5
  1.5 0.0 copy-done.1
  1.5 0.2 copy.21
  1.6 0.2 copy.22
  1.9 0.0 copy-done.4
  1.9 0.1 copy.19
  2.0 0.2 copy.20
  2.2 0.2 copy-done.5
  2.4 0.1 copy.17
  2.5 0.2 copy.18
  2.7 0.0 copy-start
  2.7 1.4 pad_maximum_fusion.w_ref
  4.1 0.0 copy-done
  4.1 0.4 copy.25
  4.5 1.6 copy.26
  6.1 0.0 copy-start.7
  6.1 0.0 copy-start.2
  6.1 0.0 copy-start.3
  6.2 109.3 %shard_map.154 = (bf16[1536,640]{1,0:T(8,128)(2,1)}, f32[4,384,192]{2,1,0:T(8,128)}) custom-call(bf16[192,4096]{1,0:T(8,128)(2,1)} %x_ref.1, f32[1,4096]{1,0:T(1,128)} %bitcast.33, bf16[4,256,640]{2,1,0:T(8,128)(2,1)} %pad_maximum_fusion.w_ref, f32[4,384,192]{2,1,0:T(8,128)} %bitcast.19), custom_call_target="tpu_custom_call" | custom-call | tf_op jit(solution)/shard_map/pallas_call | solution.py:368
  115.5 0.0 copy-done.6
  115.5 0.0 copy-done.9
  115.5 0.0 copy-done.10
  115.6 0.7 fusion.1.cpar
  116.3 0.1 concatenate.23
  116.3 0.1 reshape.42
  116.4 0.6 maximum_bitcast_fusion.rpar
  117.1 0.0 copy-done.2
  117.1 0.9 pad_maximum_fusion.1
  117.9 94.7 %shard_map.155 = bf16[192,4096]{1,0:T(8,128)(2,1)} custom-call(bf16[1536,640]{1,0:T(8,128)(2,1)} %get-tuple-element.7.proj, f32[1536,192]{1,0:T(8,128)} %bitcast.26, f32[33,128]{1,0:T(8,128)} %fusion.1.cpar, f32[4,5,192]{2,1,0:T(8,128)} %maximum_bitcast_fusion.rpar, bf16[12,64,64]{2,1,0:T(8,128)(2,1)} %dmap.1, bf16[12,64,64]{2,1,0:T(8,128)(2,1)} %imap.1, ...), custom_call_target="tpu_custom_call" | custom-call | tf_op jit(solution)/shard_map/pallas_call | solution.py:683
  212.6 2.7 %copy.29 = bf16[192,4096]{1,0:T(8,128)(2,1)} copy(bf16[192,4096]{1,0:T(8,128)(2,1)} %shard_map.155) | data formatting | bytes 3145728
  (12 shorter events, 0.0 us)
Async XLA Ops:
  0.0 1.5 copy-start.1
  0.0 1.8 copy-start.4
  1.4 1.0 copy-start.5
  2.7 1.4 copy-start
  6.1 109.4 %copy-start.6 = (bf16[31,512]{1,0:T(8,128)(2,1)S(1)}, bf16[31,512]{1,0:T(8,128)(2,1)}, u32[]{:S(2)}) copy-start(bf16[31,512]{1,0:T(8,128)(2,1)} %param.22) | copy-start | bytes 95236
  6.1 109.4 %copy-start.9 = (f32[512]{0:T(512)S(1)}, f32[512]{0:T(512)}, u32[]{:S(2)}) copy-start(f32[512]{0:T(512)} %param.23) | copy-start | bytes 6148
  6.1 109.4 %copy-start.10 = (f32[512]{0:T(512)S(1)}, f32[512]{0:T(512)}, u32[]{:S(2)}) copy-start(f32[512]{0:T(512)} %param.24) | copy-start | bytes 6148
  6.1 110.1 %copy-start.8 = (f32[768]{0:T(1024)S(1)}, f32[768]{0:T(1024)}, u32[]{:S(2)}) copy-start(f32[768]{0:T(1024)} %param.28) | copy-start | bytes 9220
  6.1 110.2 %copy-start.7 = (bf16[4,768]{1,0:T(4,128)(2,1)S(1)}, bf16[4,768]{1,0:T(4,128)(2,1)}, u32[]{:S(2)}) copy-start(bf16[4,768]{1,0:T(4,128)(2,1)} %param.25) | copy-start | bytes 18436
  6.1 110.9 %copy-start.2 = (bf16[768,256]{1,0:T(8,128)(2,1)S(1)}, bf16[768,256]{1,0:T(8,128)(2,1)}, u32[]{:S(2)}) copy-start(bf16[768,256]{1,0:T(8,128)(2,1)} %param.31) | copy-start | bytes 1179652
  6.1 110.9 %copy-start.3 = (bf16[512,256]{1,0:T(8,128)(2,1)S(1)}, bf16[512,256]{1,0:T(8,128)(2,1)}, u32[]{:S(2)}) copy-start(bf16[512,256]{1,0:T(8,128)(2,1)} %param.30) | copy-start | bytes 786436

commit v4 on v3

--- a/solution.py
+++ b/solution.py
@@ -192,6 +192,7 @@
         self.count += 1
         copy.start()
         self.open.append((copy.wait, None))
+        return self.open[-1]
 
     def arrived(self, dst, recv, device):
         pltpu.make_async_remote_copy(
@@ -274,6 +275,7 @@
     others = (me.qx, me.qy, me.qd)
     depth = w_ref.shape[1]
     rows = x_ref.shape[0]
+    jwidth = j_ref.shape[1] // 4
 
     def wslot(origin, piece):
         return wall.at[pl.ds(pl.multiple_of((origin * 4 + piece) * depth, depth), depth)]
@@ -285,7 +287,7 @@
     for q in others:
         mail.send(w_ref.at[q], wslot(me.z, me.q), rw.at[me.q], me.mate(q))
     to_line(w_ref.at[me.q], me.z, me.q)
-    mail.local(w_ref.at[me.q], wslot(me.z, me.q))
+    own_rows = mail.local(w_ref.at[me.q], wslot(me.z, me.q))
 
     first_row = (me.q * 2 + me.c) * rows
 
@@ -303,9 +305,6 @@
 
     xg = PlaneGather(me, mail, lambda h: slot(me.q, me.c, h), slot, rx, rp)
     xg.start()
-    for q in others:
-        mail.send(j_ref.at[q], jall.at[me.q], rj.at[me.q], me.mate(q))
-    mail.local(j_ref.at[me.q], jall.at[me.q])
     for q in others:
         here = wslot(me.z, q)
         mail.arrived(here, rw.at[q], me.partner)
@@ -324,14 +323,21 @@
 
     line_step(1)
     xg.first()
+
+    def share(q):
+        begin = q * jwidth // 128 * 128
+        return j_ref.at[:, pl.ds(pl.multiple_of(begin, 128), jall.shape[2])]
+
+    for q in others:
+        mail.send(share(q), jall.at[me.q], rj.at[me.q], me.mate(q))
+    mail.local(share(me.q), jall.at[me.q])
     for k in range(2, planes - 1):
         line_step(k)
     xg.second()
-    for q in others:
-        mail.arrived(jall.at[q], rj.at[q], me.partner)
     xg.third()
     xg.last()
-    mail.finish()
+    mail.open.remove(own_rows)
+    own_rows[0]()
     tile = acc.shape[0] // 4
 
     def multiply(start, size, fresh=False):
@@ -355,10 +361,18 @@
             mail.arrived(wslot(far, piece), rz.at[far, piece], me.partner)
             multiply((far * 4 + piece) * depth, depth)
 
+    for q in others:
+        mail.arrived(jall.at[q], rj.at[q], me.partner)
+    mail.finish()
+
     @pl.loop(0, 8)
     def _(i):
         part = pl.ds(pl.multiple_of(i * (tile // 2), 16), tile // 2)
         proj[part] = acc[part].astype(proj.dtype)
+
+
+def window_of(width):
+    return max(-(-(q + 1) * width // 128) * 128 - q * width // 128 * 128 for q in range(4))
 
 
 def enter(planes, tokens, gain, pieces, jumps):
@@ -369,7 +383,7 @@
         functools.partial(enter_kernel, planes),
         out_shape=(
             jax.ShapeDtypeStruct((8 * rows, cols), tokens.dtype),
-            jax.ShapeDtypeStruct(jumps.shape, jumps.dtype),
+            jax.ShapeDtypeStruct((4, jumps.shape[0], window_of(jumps.shape[1] // 4)), jumps.dtype),
         ),
         in_specs=[VMEM] * 4,
         out_specs=(VMEM,) * 2,
@@ -407,7 +421,7 @@
     f32, bf16 = jnp.float32, jnp.bfloat16
     length = proj.shape[0]
     cw = gext.shape[1]
-    rwid = jump.shape[1]
+    rwid = rpar.shape[2]
     seg = length // SEGMENTS
     top = halo.shape[0]
     fold = dec.shape[0]
@@ -472,7 +486,11 @@
         smooth = smooth.astype(bf16)
         gates = jax.nn.sigmoid(jnp.dot(smooth, maps[...], preferred_element_type=f32))
         retain, admit = gates[:, :rwid], gates[:, fold * 128 : fold * 128 + rwid]
-        log_decay = jump[pl.ds(base, seg)] - retain * softened
+        wide = jump[pl.ds(base, seg)]
+        moved = wide[:, :rwid]
+        for lead in {q * rwid % 128 for q in range(4)} - {0}:
+            moved = jnp.where(me.q * rwid % 128 == lead, wide[:, lead : lead + rwid], moved)
+        log_decay = moved - retain * softened
         decay = jnp.exp(log_decay)
         inflow = jnp.sqrt(minus_expm1(2.0 * log_decay)) * admit * smooth.astype(f32)
         for f in range(fold):
@@ -672,7 +690,7 @@
 
 
 def core(planes, proj, jump, cpar, rpar, dmap, imap, weights, lags, cw):
-    length, rwid = jump.shape
+    length, rwid = jump.shape[0], rpar.shape[2]
     used, cols = cw + rwid, weights.shape[1]
     width = used + -used % 128
     fold = (rwid + 127) // 128
@@ -741,9 +759,9 @@
         return lax.dynamic_slice_in_dim(a, q * size, size, axis)
 
     pieces = jnp.concatenate([by_mate(w) for w in (conv_val_w, conv_gate_w, rec_gate_w, rec_in_w)], axis=2)
-    projected, jall = enter(planes, tokens, norm_gain[None], pieces, by_mate(decay_jump))
+    projected, jall = enter(planes, tokens, norm_gain[None], pieces, decay_jump)
     cw, rw = conv_val_w.shape[1] // 4, rec_in_w.shape[1] // 4
-    jump = jall.reshape(-1, rw)
+    jump = jall.reshape(-1, jall.shape[2])
     cols = out_conv_w.shape[1]
     rows_by_mate = jnp.concatenate(
         [out_conv_w.reshape(4, cw, cols), out_rec_w.reshape(4, rw, cols)], axis=1

time: 216 us -> 203 us (0.940)
  Pallas kernels: 204 us -> 191 us
  other arithmetic: 3.59 us -> 5.76 us
    pallas_call x1, Pallas kernels: 109 us -> 97.1 us  [enter(): pl.pallas_call(functools.partial(enter_kernel, planes), out_shape=(jax.Sh...]
    unnamed x28 -> x15, local copies, waits for them, and re-layouts: 5 us -> 4.37 us
where the time goes in v4:
time: 203 us
  Pallas kernels  191 us (94%)
  local copies, waits for them, and re-layouts  5.99 us (3%)
  other arithmetic  5.76 us (3%)
    pallas_call x1, Pallas kernels, enter(): pl.pallas_call(functools.partial(enter_kernel, planes), out_shape=(jax.Sh...  97.1 us
    pallas_call x1, Pallas kernels, core(): pl.pallas_call(functools.partial(core_kernel, planes, lags), out_shape=ja...  94 us
    unnamed x15, local copies, waits for them, and re-layouts  4.37 us

profile of v4, /device:TPU:0, one launch (start us, length us, event | category | flops | bytes accessed | tf_op | source)
XLA Modules:
  0.0 203.0 jit_solution(17425261352360337828)
XLA Ops:
  0.0 0.0 copy-start
  0.0 0.0 copy-start.4
  0.0 0.8 fusion.2
  0.8 0.1 concatenate.23
  0.9 0.8 reshape.38
  1.6 0.6 maximum_bitcast_fusion.rpar
  2.3 0.8 convert_element_type.4
  3.0 1.3 fusion.1.cpar
  4.4 1.1 copy.17
  5.5 0.0 copy-start.1
  5.5 0.2 copy.18
  5.6 0.0 copy-done.4
  5.7 0.1 copy.19
  5.8 0.2 copy.20
  6.0 0.0 copy-done
  6.0 0.2 copy.21
  6.2 0.2 copy.22
  6.4 0.1 copy-done.1
  6.5 0.2 copy.23
  6.6 0.2 copy.24
  6.8 0.0 copy-start.2
  6.9 0.0 copy-start.3
  6.9 1.4 pad_maximum_fusion.w_ref
  8.2 0.0 copy-done.2
  8.2 0.0 copy-done.3
  8.2 0.9 pad_maximum_fusion.1
  9.1 97.1 %shard_map.154 = (bf16[1536,640]{1,0:T(8,128)(2,1)}, f32[4,384,256]{2,1,0:T(8,128)}) custom-call(bf16[192,4096]{1,0:T(8,128)(2,1)} %x_ref.1, f32[1,4096]{1,0:T(1,128)} %bitcast.29, bf16[4,256,640]{2,1,0:T(8,128)(2,1)} %pad_maximum_fusion.w_ref, f32[384,768]{1,0:T(8,128)} %j_ref.1), custom_call_target="tpu_custom_call" | custom-call | tf_op jit(solution)/shard_map/pallas_call | solution.py:382
  106.3 94.0 %shard_map.155 = bf16[192,4096]{1,0:T(8,128)(2,1)} custom-call(bf16[1536,640]{1,0:T(8,128)(2,1)} %get-tuple-element.7.proj, f32[1536,256]{1,0:T(8,128)} %bitcast.22, f32[33,128]{1,0:T(8,128)} %fusion.1.cpar, f32[4,5,192]{2,1,0:T(8,128)} %maximum_bitcast_fusion.rpar, bf16[12,64,64]{2,1,0:T(8,128)(2,1)} %dmap.1, bf16[12,64,64]{2,1,0:T(8,128)(2,1)} %imap.1, ...), custom_call_target="tpu_custom_call" | custom-call | tf_op jit(solution)/shard_map/pallas_call | solution.py:701
  200.3 2.7 %copy.27 = bf16[192,4096]{1,0:T(8,128)(2,1)} copy(bf16[192,4096]{1,0:T(8,128)(2,1)} %shard_map.155) | data formatting | bytes 3145728
  (1 shorter events, 0.0 us)
Async XLA Ops:
  0.0 6.0 %copy-start = (bf16[256,768]{1,0:T(8,128)(2,1)S(1)}, bf16[256,768]{1,0:T(8,128)(2,1)}, u32[]{:S(2)}) copy-start(bf16[256,768]{1,0:T(8,128)(2,1)} %param.20) | copy-start | bytes 1179652
  0.0 5.6 %copy-start.4 = (bf16[256,512]{1,0:T(8,128)(2,1)S(1)}, bf16[256,512]{1,0:T(8,128)(2,1)}, u32[]{:S(2)}) copy-start(bf16[256,512]{1,0:T(8,128)(2,1)} %param.19) | copy-start | bytes 786436
  5.5 1.0 copy-start.1
  6.8 1.4 copy-start.2
  6.9 1.4 copy-start.3
